TPU v7x, 512 devices: a 8x2x16 block of a 8x8x16 slice. The times are simulated.
512 devices in a mesh: grp: 2 (over y), fs: 32 (over z, core), tp: 8 (over x).
Axes of the slice: x: 8, y: 2, z: 16, core: 2. Of those that a mesh axis runs over, the one named last changes fastest.
The devices are a block of a 8x8x16 slice.
Arguments:
- tokens: bfloat16 [24576, 2048], P(('grp', 'fs'), 'tp'), parts along dimension 0, may hold values from -6 to 6
- norm_gain: float32 [2048], P('fs'), may hold values from 0.1 to 1.9
- gate_weight: float32 [32, 2048, 1024], P(None, 'fs', 'tp'), may hold values from -0.125 to 0.125
- up_weight: float32 [32, 2048, 1024], P(None, 'fs', 'tp'), may hold values from -0.125 to 0.125
- down_weight: float32 [32, 1024, 2048], P(None, 'fs', 'tp'), may hold values from -0.1875 to 0.1875
- routes: int32 [24576, 2], P(('grp', 'fs')), parts along dimension 0, may hold values from 0 to 31, as said below
- route_weights: float32 [24576, 2], P(('grp', 'fs')), parts along dimension 0, may hold values from 0.2 to 1
Outputs:
- gate_serve: bfloat16 [64, 2048, 1024], P(('grp', 'fs'), None, 'tp'), parts along dimension 0
- up_serve: bfloat16 [64, 2048, 1024], P(('grp', 'fs'), None, 'tp'), parts along dimension 0
- down_serve: bfloat16 [64, 1024, 2048], P(('grp', 'fs'), None, 'tp'), parts along dimension 0
- mixture: bfloat16 [24576, 2048], P(('grp', 'fs'), 'tp'), parts along dimension 0
There are 2 independent parts, one for each index of `grp`. A program takes and returns all parts, laid end to end along the dimension named above; an argument that names none is the same for every part. Nothing has to cross between parts.
Inputs may be any that keep to these rules, and one draw needn't show every extreme that they name: `routes`: each row names two different experts of one group (expert e lies in group e // 8). In each aligned block of 384 rows no expert is named more than 36 times, and every expert of one group is named exactly 36 times.
All inputs are finite; a program needn't handle non-finite values.
Results may differ from a plain program's by a relative error of at most 0.0087.
Values may be sent and summed in bfloat16 or wider, within the bound.
A program may use at most 64 MiB of HBM per device.

v0:
```python
import jax
import jax.numpy as jnp
from jax import lax
from jax.sharding import Mesh
from jax.sharding import PartitionSpec as P

CAP = 36
FS = ("fs_0", "fs_1")
GRP_FS = ("grp", "fs_0", "fs_1")


epsilon = 1e-06


def in_blocks(x, dim, length):
    before, after = (x.shape[:dim], x.shape[dim + 1 :])
    return jnp.moveaxis(x.reshape(*before, length, -1, *after), dim, 0)


def laid_out(blocks, dim):
    blocks = jnp.moveaxis(blocks, 0, dim)
    shape = blocks.shape
    return blocks.reshape(*shape[:dim], shape[dim] * shape[dim + 1], *shape[dim + 2 :])


def exchange_in_order(blocks, axes, order):
    shape = [lax.axis_size(a) for a in axes]
    blocks = blocks.reshape(*shape, *blocks.shape[1:])
    for k in order:
        blocks = lax.all_to_all(blocks, axes[k], split_axis=k, concat_axis=k, tiled=True)
    return blocks.reshape(-1, *blocks.shape[len(axes) :])


def exchange_by_chip(x, groups, order, split_dim, concat_dim):
    length = lax.axis_size(groups[0]) * lax.axis_size(groups[1])
    blocks = in_blocks(x, split_dim, length)
    return laid_out(exchange_in_order(blocks, groups, order), concat_dim)


def normalize(rows):
    values = rows.astype(jnp.float32)
    scale = lax.rsqrt(jnp.mean(values * values, axis=-1, keepdims=True) + epsilon)
    return (values * scale).astype(jnp.bfloat16)


def shards(tokens, norm_gain, gate_weight, up_weight, down_weight, routes, route_weights):
    experts = gate_weight.shape[0]
    n_shards = lax.axis_size(FS)
    local_experts = experts // n_shards
    tok_rows = tokens.shape[0]
    gate_low = (norm_gain[None, :, None] * gate_weight).astype(jnp.bfloat16)
    up_low = (norm_gain[None, :, None] * up_weight).astype(jnp.bfloat16)
    down_low = down_weight.astype(jnp.bfloat16)
    gate_serve, up_serve = (
        lax.all_to_all(gate_low, FS, split_axis=0, concat_axis=1, tiled=True),
        lax.all_to_all(up_low, FS, split_axis=0, concat_axis=1, tiled=True),
    )
    flat_routes = routes.reshape(-1)
    expert_ids = lax.iota(jnp.int32, experts)
    onehot = (flat_routes[:, None] == expert_ids[None, :]).astype(jnp.int32)
    position = jnp.sum((jnp.cumsum(onehot, axis=0) - 1) * onehot, axis=1)
    slot_index = (flat_routes * CAP + position).reshape(tok_rows, 2)
    slot_ids = lax.iota(jnp.int32, experts * CAP)
    select = jnp.any(slot_ids[:, None, None] == slot_index[None, :, :], axis=2).astype(jnp.bfloat16)
    outbound = jnp.dot(select, tokens, preferred_element_type=jnp.float32).astype(jnp.bfloat16)
    outbound = outbound.reshape(n_shards, local_experts, CAP, outbound.shape[1])
    arrived = lax.all_to_all(outbound, FS, split_axis=0, concat_axis=2, tiled=True)[0]
    expert_rows = normalize(lax.all_gather(arrived, "tp", axis=2, tiled=True))
    gate_part = jnp.einsum(
        "erd,edh->erh", expert_rows, gate_serve, preferred_element_type=jnp.float32
    )
    up_part = jnp.einsum("erd,edh->erh", expert_rows, up_serve, preferred_element_type=jnp.float32)
    hidden = (jax.nn.silu(gate_part) * up_part).astype(jnp.bfloat16)
    down_serve = lax.all_to_all(down_low, FS, split_axis=0, concat_axis=1, tiled=True)
    expert_out = jnp.einsum(
        "erk,ekd->erd",
        lax.all_gather(hidden, "tp", axis=2, tiled=True),
        down_serve,
        preferred_element_type=jnp.float32,
    ).astype(jnp.bfloat16)
    expert_out = expert_out.reshape(1, local_experts, hidden.shape[1], expert_out.shape[2])
    returned_rows = exchange_by_chip(expert_out, ("fs_0", "fs_1"), (1, 0), 2, 0)
    returned_rows = returned_rows.reshape(experts * CAP, returned_rows.shape[3])
    picked = returned_rows[slot_index]
    mixture = jnp.sum(route_weights[:, :, None] * picked.astype(jnp.float32), axis=1).astype(
        jnp.bfloat16
    )
    return (gate_serve, up_serve, down_serve, mixture)


def solution(mesh):
    split = Mesh(
        mesh.devices.reshape(mesh.shape["grp"], 16, 2, mesh.shape["tp"]),
        ("grp", "fs_0", "fs_1", "tp"),
    )
    placed = (
        P(GRP_FS, "tp"),
        P(FS),
        P(None, FS, "tp"),
        P(None, FS, "tp"),
        P(None, FS, "tp"),
        P(GRP_FS, None),
        P(GRP_FS, None),
    )
    return jax.shard_map(
        shards,
        mesh=split,
        in_specs=placed,
        out_specs=(
            P(GRP_FS, None, "tp"),
            P(GRP_FS, None, "tp"),
            P(GRP_FS, None, "tp"),
            P(GRP_FS, "tp"),
        ),
        check_vma=False,
    )
```

profile of v0, /device:TPU:65, one launch (start us, length us, event | category | flops | bytes accessed | tf_op | source)
XLA Modules:
  0.0 289.2 jit_solution(14518242084303444602)
XLA Ops:
  7.3 0.9 copy.41
  8.5 1.7 reduce-window.6
  10.3 0.3 slice_reduce_fusion
  10.7 0.2 reduce_sum.30
  10.9 0.7 compare_select_fusion
  11.6 0.8 fusion.3
  12.4 0.5 convolution_convert_fusion.1
  13.0 83.8 %all_to_all.55 = bf16[32,1,36,256]{3,2,1,0:T(8,128)(2,1)S(1)} all-to-all(bf16[32,1,36,256]{3,2,1,0:T(8,128)(2,1)S(1)} %bitcast.35), channel_id=1, replica_groups=mesh['grp'=2,'fs_0'=16,'fs_1'=2,'tp'=8] {'fs_0','fs_1'}, dimensions={0} | all-to-all | bytes 1179648 | tf_op jit(solution)/shard_map/all_to_all | solution.py:67
  96.8 0.9 squeeze.3
  97.9 2.3 multiply_convert_fusion
  100.2 36.8 %all_to_all.56 = bf16[32,64,128]{2,1,0:T(8,128)(2,1)S(1)} all-to-all(bf16[32,64,128]{2,1,0:T(8,128)(2,1)S(1)} %get-tuple-element.7), channel_id=1, replica_groups=mesh['grp'=2,'fs_0'=16,'fs_1'=2,'tp'=8] {'fs_0','fs_1'}, dimensions={0} | all-to-all | bytes 1048576 | tf_op jit(solution)/shard_map/all_to_all | solution.py:55
  137.0 4.5 %all-to-all-start.1 = ((bf16[32,64,128]{2,1,0:T(8,128)(2,1)}), bf16[32,64,128]{2,1,0:T(8,128)(2,1)S(1)}, u32[]{:S(2)}, u32[]{:S(2)}) async-start(bf16[32,64,128]{2,1,0:T(8,128)(2,1)} %get-tuple-element.6), calls=%async_computation.1 | async-start | bytes 1048576 | tf_op jit(solution)/shard_map/all_to_all | solution.py:56
  141.6 18.2 %all-gather.4.cloned.1.call-done = bf16[1,1152,2048]{2,1,0:T(8,128)(2,1)} async-done(((bf16[1,1152,256]{2,1,0:T(8,128)(2,1)}), bf16[1,1152,2048]{2,1,0:T(8,128)(2,1)}) %all-gather.4.cloned.1.call-update) | async-done | bytes 4718608 | tf_op jit(solution)/shard_map/all_gather | solution.py:68
  159.8 3.5 %fusion = f32[1152]{0:T(1024)S(1)} fusion(bf16[1,1152,2048]{2,1,0:T(8,128)(2,1)} %all-gather.4.cloned.1.call-done), kind=kLoop, calls=%fused_computation.3 | loop fusion | flops 7076736 | bytes 4723200 | tf_op jit(solution)/shard_map/reduce_sum | solution.py:42
  163.3 0.3 copy-done.1
  163.6 1.5 fusion.6
  165.0 9.9 %all-to-all-done.1 = bf16[32,64,128]{2,1,0:T(8,128)(2,1)S(1)} async-done(((bf16[32,64,128]{2,1,0:T(8,128)(2,1)}), bf16[32,64,128]{2,1,0:T(8,128)(2,1)S(1)}, u32[]{:S(2)}, u32[]{:S(2)}) %all-to-all-start.1) | async-done | bytes 524320 | tf_op jit(solution)/shard_map/all_to_all | solution.py:56
  174.9 4.6 %fusion.4 = bf16[1152,128]{1,0:T(8,128)(2,1)} fusion(bf16[2048,128]{1,0:T(8,128)(2,1)S(1)} %bitcast.38, bf16[1,1152,2048]{2,1,0:T(8,128)(2,1)} %all-gather.4.cloned.1.call-done, f32[1152]{0:T(1024)S(1)} %add_rsqrt_fusion, f32[1152,128]{1,0:T(8,128)S(1)} %fusion.6), kind=kOutput, calls=%fused_computation.11 | convolution fusion | flops 611942400 | bytes 6132224 | tf_op jit(solution)/shard_map/erd,edh->erh/dot_general | solution.py:72
  179.7 40.3 %all_to_all.57 = bf16[32,32,256]{2,1,0:T(8,128)(2,1)S(1)} all-to-all(bf16[32,32,256]{2,1,0:T(8,128)(2,1)S(1)} %convert_element_type.42), channel_id=1, replica_groups=mesh['grp'=2,'fs_0'=16,'fs_1'=2,'tp'=8] {'fs_0','fs_1'}, dimensions={0} | all-to-all | bytes 1048576 | tf_op jit(solution)/shard_map/all_to_all | solution.py:74
  220.0 3.7 %all-gather.6.cloned.1.call-done = bf16[1152,1024]{1,0:T(8,128)(2,1)} async-done(((bf16[1152,128]{1,0:T(8,128)(2,1)}), bf16[1152,1024]{1,0:T(8,128)(2,1)}) %all-gather.6.cloned.1.call-update) | async-done | bytes 2359312 | tf_op jit(solution)/shard_map/all_gather | solution.py:77
  223.6 2.4 convolution_convert_fusion
  226.2 0.2 copy.46
  226.4 10.4 %all_to_all.58 = bf16[16,2,1,1,36,256]{5,0,4,3,2,1:T(8,128)(2,1)S(1)} all-to-all(bf16[16,2,1,1,36,256]{5,0,4,3,2,1:T(8,128)(2,1)S(1)} %copy.46), channel_id=1, replica_groups=mesh['grp'=2,'fs_0'=16,'fs_1'=2,'tp'=8] {'fs_1'}, dimensions={1} | all-to-all | bytes 1179648 | tf_op jit(solution)/shard_map/all_to_all | solution.py:30
  236.8 1.4 copy.47
  238.2 11.2 %all-to-all-start.5 = ((bf16[16,2,1,1,36,256]{5,1,4,3,2,0:T(2,128)(2,1)}), bf16[16,2,1,1,36,256]{5,1,4,3,2,0:T(2,128)(2,1)S(1)}, u32[]{:S(2)}, u32[]{:S(2)}) async-start(bf16[16,2,1,1,36,256]{5,1,4,3,2,0:T(2,128)(2,1)} %copy.47), calls=%async_computation.5 | async-start | bytes 1179648 | tf_op jit(solution)/shard_map/all_to_all | solution.py:30
  249.8 25.2 %all-to-all-done.5 = bf16[16,2,1,1,36,256]{5,1,4,3,2,0:T(2,128)(2,1)S(1)} async-done(((bf16[16,2,1,1,36,256]{5,1,4,3,2,0:T(2,128)(2,1)}), bf16[16,2,1,1,36,256]{5,1,4,3,2,0:T(2,128)(2,1)S(1)}, u32[]{:S(2)}, u32[]{:S(2)}) %all-to-all-start.5) | async-done | bytes 589856 | tf_op jit(solution)/shard_map/all_to_all | solution.py:30
  275.2 2.7 gather_fusion
  277.8 0.4 reshape.117
  278.2 1.7 multiply_reduce_fusion
  280.0 0.8 copy.55
  280.8 0.8 copy.56
  281.5 0.8 copy.57
  (31 shorter events, 1.7 us)
Async XLA Ops:
  7.2 5.2 %copy-start = (bf16[384,256]{1,0:T(8,128)(2,1)S(1)}, bf16[384,256]{1,0:T(8,128)(2,1)}, u32[]{:S(2)}) copy-start(bf16[384,256]{1,0:T(8,128)(2,1)} %param.7) | copy-start | bytes 589828
  7.2 90.7 %copy-start.3 = (f32[32,64,128]{2,1,0:T(8,128)S(1)}, f32[32,64,128]{2,1,0:T(8,128)}, u32[]{:S(2)}) copy-start(f32[32,64,128]{2,1,0:T(8,128)} %param.10) | copy-start | bytes 3145732
  7.2 90.7 %copy-start.5 = (f32[64]{0:T(128)S(1)}, f32[64]{0:T(128)}, u32[]{:S(2)}) copy-start(f32[64]{0:T(128)} %param.8) | copy-start | bytes 772
  7.2 152.6 %all-gather.4.cloned.1.call-start = ((), (), s32[]{:S(2)}) async-start(), calls=%async_computation.6 | async-start | bytes 5308416 | tf_op jit(solution)/shard_map/all_gather | solution.py:68
  137.0 38.0 %all-to-all-start.1 = ((bf16[32,64,128]{2,1,0:T(8,128)(2,1)}), bf16[32,64,128]{2,1,0:T(8,128)(2,1)S(1)}, u32[]{:S(2)}, u32[]{:S(2)}) async-start(bf16[32,64,128]{2,1,0:T(8,128)(2,1)} %get-tuple-element.6), calls=%async_computation.1 | async-start | bytes 1048576 | tf_op jit(solution)/shard_map/all_to_all | solution.py:56
  141.5 82.1 %all-gather.6.cloned.1.call-start = ((), (), s32[]{:S(2)}) async-start(), calls=%async_computation.7 | async-start | bytes 2654208 | tf_op jit(solution)/shard_map/all_gather | solution.py:77
  159.8 3.8 %copy-start.1 = (bf16[1,1152,2048]{2,1,0:T(8,128)(2,1)S(1)}, bf16[1,1152,2048]{2,1,0:T(8,128)(2,1)}, u32[]{:S(2)}) copy-start(bf16[1,1152,2048]{2,1,0:T(8,128)(2,1)} %all-gather.4.cloned.1.call-done) | copy-start | bytes 14155780
  174.9 4.7 %copy-start.2 = (f32[32,32,256]{2,1,0:T(8,128)S(1)}, f32[32,32,256]{2,1,0:T(8,128)}, u32[]{:S(2)}) copy-start(f32[32,32,256]{2,1,0:T(8,128)} %param.11) | copy-start | bytes 3145732
  226.1 23.6 %copy-start.4 = (f32[384,2]{0,1:T(2,128)S(1)}, f32[384,2]{0,1:T(2,128)}, u32[]{:S(2)}) copy-start(f32[384,2]{0,1:T(2,128)} %param.13) | copy-start | bytes 9220
  238.2 36.8 %all-to-all-start.5 = ((bf16[16,2,1,1,36,256]{5,1,4,3,2,0:T(2,128)(2,1)}), bf16[16,2,1,1,36,256]{5,1,4,3,2,0:T(2,128)(2,1)S(1)}, u32[]{:S(2)}, u32[]{:S(2)}) async-start(bf16[16,2,1,1,36,256]{5,1,4,3,2,0:T(2,128)(2,1)} %copy.47), calls=%async_computation.5 | async-start | bytes 1179648 | tf_op jit(solution)/shard_map/all_to_all | solution.py:30
Sparse Core Ops, SparseCore 0:
  98.0 61.7 all-gather.3
  179.7 43.8 all-gather.5
where the time goes:
time: 294 us; the launch traced here: 289 us
  blocking collectives  171 us (58%)
  waiting for transfers between devices  57.1 us (19%)
  starting transfers between devices  15.8 us (5%)
  between operations  14.3 us (5%)
  other arithmetic  10.9 us (4%)
  local copies, waits for them, and re-layouts  10.8 us (4%)
  matrix products  8.97 us (3%)
    all_to_all x1, blocking collectives, shards(): lax.all_to_all(outbound, FS, split_axis=0, concat_axis=2, tiled=True)[0]  83.8 us
    all_to_all x1, blocking collectives, shards(): lax.all_to_all(down_low, FS, split_axis=0, concat_axis=1, tiled=True)  40.3 us
    all_to_all x1, blocking collectives, shards(): lax.all_to_all(gate_low, FS, split_axis=0, concat_axis=1, tiled=True)  36.8 us
    all_to_all x1, waiting for transfers between devices, exchange_in_order(): lax.all_to_all(blocks, axes[k], split_axis=k, concat_axis=k, tiled=True)  25.2 us
    all_gather x1, waiting for transfers between devices, shards(): expert_rows = normalize(lax.all_gather(arrived, 'tp', axis=2, tiled=True))  18.2 us
    all_to_all x1, starting transfers between devices, exchange_in_order(): lax.all_to_all(blocks, axes[k], split_axis=k, concat_axis=k, tiled=True)  11.2 us
    all_to_all x1, blocking collectives, exchange_in_order(): lax.all_to_all(blocks, axes[k], split_axis=k, concat_axis=k, tiled=True)  10.4 us
    all_to_all x1, waiting for transfers between devices, shards(): lax.all_to_all(up_low, FS, split_axis=0, concat_axis=1, tiled=True)  9.9 us
  transfers between devices with their start and end apart: 4, of which 4 were waited for; matrix products, arithmetic and copies ran while one was open for 3% of the time, Pallas kernels for 0%

commit v1 on v0

v1 whole, which is shorter than its diff:
```python
import functools

import jax
import jax.numpy as jnp
from jax import lax
from jax.experimental import pallas as pl
from jax.experimental.pallas import tpu as pltpu
from jax.sharding import Mesh
from jax.sharding import PartitionSpec as P

CAP = 36
FS = ("fs_0", "fs_1")
GRP_FS = ("grp", "fs_0", "fs_1")
MESH = pl.DeviceIdType.MESH
EPSILON = 1e-06
CHUNKS = 4


def ring_order(n):
    order = [0]
    for d in range(1, n // 2 + 1):
        order.append(d)
        if len(order) < n:
            order.append(n - d)
    return order


def kernel(
    sizes,
    gate_ref,
    up_ref,
    down_ref,
    outb_ref,
    gate_out,
    up_out,
    down_out,
    ret_ref,
    swap,
    comb,
    x_buf,
    h_buf,
    o_buf,
    gate_v,
    up_v,
    down_v,
    swap_sems,
    tok_s,
    tok_r,
    gu_s,
    gu_r,
    dn_s,
    dn_r,
    ygu_s,
    ygu_r,
    ydn_s,
    ydn_r,
    xs,
    xr,
    hs,
    hr,
    ret_s,
    ret_r,
    fin_s,
    fin_r,
    out_sem,
):
    n_z, n_x, n_grp = sizes
    order = ring_order(n_z)
    per = n_z // CHUNKS
    slot, width = x_buf.shape[2], x_buf.shape[3]
    g_half = gate_v.shape[1] // 2
    d_half = down_v.shape[1] // 2
    grp = lax.axis_index("grp")
    z = lax.axis_index("fs_0")
    core = lax.axis_index("fs_1")
    x = lax.axis_index("tp")
    me = z * 2 + core
    half = lax.rem(grp, 2)
    y_peer = {"grp": grp + 1 - 2 * half}
    other_core = {"fs_1": 1 - core}
    right = {"tp": lax.rem(x + 1, n_x)}
    left = {"tp": lax.rem(x + n_x - 1, n_x)}
    sends = []

    def ahead(pos):
        return lax.rem(z + order[pos], n_z)

    def behind(pos):
        return lax.rem(z + n_z - order[pos], n_z)

    def remote(src, dst, send_sem, recv_sem, device):
        return pltpu.make_async_remote_copy(
            src_ref=src, dst_ref=dst, send_sem=send_sem, recv_sem=recv_sem, device_id=device, device_id_type=MESH
        )

    def send(*args):
        copy = remote(*args)
        copy.start()
        sends.append(copy)
        return copy

    barrier = pltpu.get_barrier_semaphore()
    peers = [y_peer, other_core, right, left]
    for pos in range(1, n_z):
        for c in range(2):
            peers.append({"fs_0": ahead(pos), "fs_1": c})
    for device in peers:
        pl.semaphore_signal(barrier, inc=1, device_id=device, device_id_type=MESH)
    pl.semaphore_wait(barrier, len(peers))

    first = send(outb_ref.at[1], swap, swap_sems.at[0], swap_sems.at[1], other_core)
    first.wait_recv()
    comb[...] = outb_ref[0] + swap[...]
    x_buf[0, 0] = outb_ref[0, 0] + swap[0]

    for pos in range(1, n_z):
        send(comb.at[pos], x_buf.at[0, pos], tok_s.at[pos], tok_r.at[pos], {"fs_0": ahead(pos)})

    g_rows = pl.ds(pl.multiple_of(half * g_half, g_half), g_half)
    d_rows = pl.ds(pl.multiple_of(half * d_half, d_half), d_half)
    gate_v[me] = gate_ref[me]
    up_v[me] = up_ref[me]
    down_v[me] = down_ref[me]
    mate = z * 2 + 1 - core
    send(gate_ref.at[mate], gate_v.at[me], gu_s.at[0, 0, 0], gu_r.at[0, 0, 0], other_core)
    send(up_ref.at[mate], up_v.at[me], gu_s.at[0, 0, 1], gu_r.at[0, 0, 1], other_core)
    send(down_ref.at[mate], down_v.at[me], dn_s.at[0, 0], dn_r.at[0, 0], other_core)
    for pos in range(1, n_z):
        for c in range(2):
            cc = lax.rem(core + c, 2)
            e = ahead(pos) * 2 + cc
            device = {"fs_0": ahead(pos), "fs_1": cc}
            send(gate_ref.at[e, g_rows], gate_v.at[me, g_rows], gu_s.at[pos, c, 0], gu_r.at[pos, c, 0], device)
            send(up_ref.at[e, g_rows], up_v.at[me, g_rows], gu_s.at[pos, c, 1], gu_r.at[pos, c, 1], device)
    for pos in range(1, n_z):
        for c in range(2):
            cc = lax.rem(core + c, 2)
            e = ahead(pos) * 2 + cc
            device = {"fs_0": ahead(pos), "fs_1": cc}
            send(down_ref.at[e, d_rows], down_v.at[me, d_rows], dn_s.at[pos, c], dn_r.at[pos, c], device)

    def got(ref, sem):
        pltpu.make_async_copy(ref, ref, sem).wait()

    def wait_tokens(k):
        for pos in range(k * per, (k + 1) * per):
            if pos:
                got(x_buf.at[0, pos], tok_r.at[pos])

    def hop(buf, k, h, s_sems, r_sems):
        whole = pl.ds(k * per, per)
        first_half, second_half = pl.ds(k * per, per // 2), pl.ds(k * per + per // 2, per // 2)
        last = n_x // 2
        if h > 1:
            arrived(buf, k, h - 1, r_sems)
        rows = first_half if h == last else whole
        send(buf.at[h - 1, rows], buf.at[h, rows], s_sems.at[k, h - 1, 0], r_sems.at[k, h - 1, 0], right)
        rows = second_half if h == last else whole
        send(buf.at[(n_x - h + 1) % n_x, rows], buf.at[n_x - h, rows], s_sems.at[k, h - 1, 1], r_sems.at[k, h - 1, 1], left)

    def arrived(buf, k, h, r_sems):
        last = n_x // 2
        whole = pl.ds(k * per, per)
        first_half, second_half = pl.ds(k * per, per // 2), pl.ds(k * per + per // 2, per // 2)
        got(buf.at[h, first_half if h == last else whole], r_sems.at[k, h - 1, 0])
        got(buf.at[n_x - h, second_half if h == last else whole], r_sems.at[k, h - 1, 1])

    def forward_gu(k):
        for pos in range(max(1, k * per), (k + 1) * per):
            for c in range(2):
                cc = lax.rem(core + c, 2)
                s = behind(pos) * 2 + cc
                got(gate_v.at[s, g_rows], gu_r.at[pos, c, 0])
                got(up_v.at[s, g_rows], gu_r.at[pos, c, 1])
            pair = pl.ds(behind(pos) * 2, 2)
            send(gate_v.at[pair, g_rows], gate_v.at[pair, g_rows], ygu_s.at[pos, 0], ygu_r.at[pos, 0], y_peer)
            send(up_v.at[pair, g_rows], up_v.at[pair, g_rows], ygu_s.at[pos, 1], ygu_r.at[pos, 1], y_peer)

    def forward_dn(k):
        for pos in range(max(1, k * per), (k + 1) * per):
            for c in range(2):
                cc = lax.rem(core + c, 2)
                got(down_v.at[behind(pos) * 2 + cc, d_rows], dn_r.at[pos, c])
            pair = pl.ds(behind(pos) * 2, 2)
            send(down_v.at[pair, d_rows], down_v.at[pair, d_rows], ydn_s.at[pos], ydn_r.at[pos], y_peer)

    def hop_x(k, h):
        if h == 1:
            wait_tokens(k)
        hop(x_buf, k, h, xs, xr)

    hop_x(0, 1)
    hop_x(1, 1)
    hop_x(0, 2)
    hop_x(1, 2)
    hop_x(0, 3)
    hop_x(1, 3)
    hop_x(2, 1)
    hop_x(0, 4)
    hop_x(1, 4)
    hop_x(3, 1)
    hop_x(2, 2)
    hop_x(3, 2)
    forward_gu(0)
    hop_x(2, 3)
    forward_gu(1)
    hop_x(3, 3)
    forward_gu(2)
    hop_x(2, 4)
    hop_x(3, 4)
    forward_gu(3)

    o_g_rows = pl.ds(pl.multiple_of((1 - half) * g_half, g_half), g_half)
    o_d_rows = pl.ds(pl.multiple_of((1 - half) * d_half, d_half), d_half)
    got(gate_v.at[mate], gu_r.at[0, 0, 0])
    got(up_v.at[mate], gu_r.at[0, 0, 1])
    for pos in range(1, n_z):
        pair = pl.ds(behind(pos) * 2, 2)
        got(gate_v.at[pair, o_g_rows], ygu_r.at[pos, 0])
        got(up_v.at[pair, o_g_rows], ygu_r.at[pos, 1])
    outs = [
        pltpu.make_async_copy(gate_v, gate_out, out_sem.at[0]),
        pltpu.make_async_copy(up_v, up_out, out_sem.at[1]),
        pltpu.make_async_copy(down_v, down_out, out_sem.at[2]),
    ]
    outs[0].start()
    outs[1].start()

    f_src = 2 * n_z // n_x
    rows = per * slot

    def expert_hidden(k):
        for h in ((4,) if k < 2 else (4,)):
            arrived(x_buf, k, h, xr)
        total = jnp.zeros((rows, 2 * gate_v.shape[2]), jnp.float32)
        square = jnp.zeros((rows, width), jnp.float32)
        for s in range(n_x):
            t = lax.rem(x + n_x - s, n_x)
            block = x_buf[s, k * per : (k + 1) * per].reshape(rows, width)
            src = pl.ds(t * f_src, f_src)
            w = jnp.concatenate(
                [gate_v[src].reshape(width, gate_v.shape[2]), up_v[src].reshape(width, up_v.shape[2])], axis=1
            )
            total = total + jnp.dot(block, w, preferred_element_type=jnp.float32)
            wide = block.astype(jnp.float32)
            square = square + wide * wide
        scale = lax.rsqrt(jnp.sum(square, axis=1, keepdims=True) * (1.0 / (n_x * width)) + EPSILON)
        n_h = gate_v.shape[2]
        g = total[:, :n_h] * scale
        u = total[:, n_h:] * scale
        hidden = (g / (1.0 + jnp.exp(-g))) * u
        h_buf[0, k * per : (k + 1) * per] = hidden.astype(jnp.bfloat16).reshape(per, slot, n_h)

    def hop_h(k, h):
        hop(h_buf, k, h, hs, hr)

    def expert_out(k):
        arrived(h_buf, k, 4, hr)
        n_h = h_buf.shape[3]
        total = jnp.zeros((rows, width), jnp.float32)
        for s in range(n_x):
            t = lax.rem(x + n_x - s, n_x)
            w = down_v[pl.ds(t * f_src, f_src)].reshape(n_h, width)
            block = h_buf[s, k * per : (k + 1) * per].reshape(rows, n_h)
            total = total + jnp.dot(block, w, preferred_element_type=jnp.float32)
        o_buf[k * per : (k + 1) * per] = total.astype(jnp.bfloat16).reshape(per, slot, width)

    def send_out(k):
        for pos in reversed(range(k * per, (k + 1) * per)):
            if pos:
                send(o_buf.at[pos], ret_ref.at[0, pos], ret_s.at[pos], ret_r.at[pos], {"fs_0": behind(pos)})
            else:
                ret_ref[0, 0] = o_buf[0]

    expert_hidden(3)
    hop_h(3, 1)
    expert_hidden(2)
    hop_h(2, 1)
    hop_h(3, 2)
    expert_hidden(1)
    hop_h(2, 2)
    hop_h(3, 3)
    hop_h(1, 1)
    hop_h(2, 3)
    expert_hidden(0)
    hop_h(3, 4)
    hop_h(2, 4)
    hop_h(0, 1)
    hop_h(1, 2)
    for k in range(CHUNKS):
        forward_dn(k)
    hop_h(0, 2)
    hop_h(1, 3)
    got(down_v.at[mate], dn_r.at[0, 0])
    for pos in range(1, n_z):
        got(down_v.at[pl.ds(behind(pos) * 2, 2), o_d_rows], ydn_r.at[pos])
    outs[2].start()
    expert_out(3)
    send_out(3)
    hop_h(0, 3)
    hop_h(1, 4)
    expert_out(2)
    send_out(2)
    hop_h(0, 4)
    expert_out(1)
    send_out(1)
    expert_out(0)
    send_out(0)

    for k in reversed(range(CHUNKS)):
        part = pl.ds(k * per, per)
        for pos in range(k * per, (k + 1) * per):
            if pos:
                got(ret_ref.at[0, pos], ret_r.at[pos])
        send(ret_ref.at[0, part], ret_ref.at[1, part], fin_s.at[k], fin_r.at[k], other_core)
    for k in reversed(range(CHUNKS)):
        got(ret_ref.at[1, pl.ds(k * per, per)], fin_r.at[k])
    for copy in outs:
        copy.wait()
    for copy in sends:
        copy.wait_send()


def exchange_and_apply(gate_low, up_low, down_low, outb, sizes):
    n_z, n_x, n_grp = sizes
    bf16 = jnp.bfloat16
    _, _, slot, width = outb.shape
    n_h = gate_low.shape[2]
    dma = pltpu.SemaphoreType.DMA
    hops = n_x // 2
    vmem = pl.BlockSpec(memory_space=pltpu.VMEM)
    hbm = pl.BlockSpec(memory_space=pl.ANY)
    return pl.pallas_call(
        functools.partial(kernel, sizes),
        out_shape=(
            jax.ShapeDtypeStruct(gate_low.shape, bf16),
            jax.ShapeDtypeStruct(up_low.shape, bf16),
            jax.ShapeDtypeStruct(down_low.shape, bf16),
            jax.ShapeDtypeStruct(outb.shape, bf16),
        ),
        in_specs=[vmem] * 4,
        out_specs=(hbm, hbm, hbm, vmem),
        scratch_shapes=[
            pltpu.VMEM(outb.shape[1:], bf16),
            pltpu.VMEM(outb.shape[1:], bf16),
            pltpu.VMEM((n_x, n_z, slot, width), bf16),
            pltpu.VMEM((n_x, n_z, slot, n_h), bf16),
            pltpu.VMEM(outb.shape[1:], bf16),
            pltpu.VMEM(gate_low.shape, bf16),
            pltpu.VMEM(up_low.shape, bf16),
            pltpu.VMEM(down_low.shape, bf16),
            dma((2,)),
            dma((n_z,)),
            dma((n_z,)),
            dma((n_z, 2, 2)),
            dma((n_z, 2, 2)),
            dma((n_z, 2)),
            dma((n_z, 2)),
            dma((n_z, 2)),
            dma((n_z, 2)),
            dma((n_z,)),
            dma((n_z,)),
            dma((CHUNKS, hops, 2)),
            dma((CHUNKS, hops, 2)),
            dma((CHUNKS, hops, 2)),
            dma((CHUNKS, hops, 2)),
            dma((n_z,)),
            dma((n_z,)),
            dma((CHUNKS,)),
            dma((CHUNKS,)),
            dma((3,)),
        ],
        compiler_params=pltpu.CompilerParams(
            collective_id=0, has_side_effects=True, vmem_limit_bytes=40 * 1024 * 1024
        ),
        name="exchange_and_apply",
    )(gate_low, up_low, down_low, outb)


def shards(tokens, norm_gain, gate_weight, up_weight, down_weight, routes, route_weights):
    experts = gate_weight.shape[0]
    n_z = lax.axis_size("fs_0")
    n_x = lax.axis_size("tp")
    n_grp = lax.axis_size("grp")
    tok_rows, width = tokens.shape
    gate_low = (norm_gain[None, :, None] * gate_weight).astype(jnp.bfloat16)
    up_low = (norm_gain[None, :, None] * up_weight).astype(jnp.bfloat16)
    down_low = down_weight.astype(jnp.bfloat16)

    flat_routes = routes.reshape(-1)
    expert_ids = lax.iota(jnp.int32, experts)
    onehot = (flat_routes[:, None] == expert_ids[None, :]).astype(jnp.int32)
    position = jnp.sum((jnp.cumsum(onehot, axis=0) - 1) * onehot, axis=1)
    order = ring_order(n_z)
    distance = lax.rem(flat_routes // 2 - lax.axis_index("fs_0") + n_z, n_z)
    pos = jnp.where(distance == 0, 0, jnp.where(distance <= n_z // 2, 2 * distance - 1, 2 * (n_z - distance)))
    crossed = jnp.abs(lax.rem(flat_routes, 2) - lax.axis_index("fs_1"))
    slots = 2 * CAP
    slot_index = (crossed * (n_z * slots + CAP) + pos * slots + position).reshape(tok_rows, 2)
    slot_ids = lax.iota(jnp.int32, 2 * n_z * slots)
    select = jnp.any(slot_ids[:, None, None] == slot_index[None, :, :], axis=2).astype(jnp.bfloat16)
    outbound = jnp.dot(select, tokens, preferred_element_type=jnp.float32).astype(jnp.bfloat16)
    outbound = outbound.reshape(2, n_z, slots, width)
    gate_serve, up_serve, down_serve, back = exchange_and_apply(
        gate_low, up_low, down_low, outbound, (n_z, n_x, n_grp)
    )
    picked = back.reshape(2 * n_z * slots, width)[slot_index]
    mixture = jnp.sum(route_weights[:, :, None] * picked.astype(jnp.float32), axis=1).astype(
        jnp.bfloat16
    )
    return (
        gate_serve.reshape(1, -1, gate_serve.shape[2]),
        up_serve.reshape(1, -1, up_serve.shape[2]),
        down_serve.reshape(1, -1, down_serve.shape[2]),
        mixture,
    )


def solution(mesh):
    split = Mesh(
        mesh.devices.reshape(mesh.shape["grp"], mesh.shape["fs"] // 2, 2, mesh.shape["tp"]),
        ("grp", "fs_0", "fs_1", "tp"),
    )
    placed = (
        P(GRP_FS, "tp"),
        P(FS),
        P(None, FS, "tp"),
        P(None, FS, "tp"),
        P(None, FS, "tp"),
        P(GRP_FS, None),
        P(GRP_FS, None),
    )
    return jax.shard_map(
        shards,
        mesh=split,
        in_specs=placed,
        out_specs=(
            P(GRP_FS, None, "tp"),
            P(GRP_FS, None, "tp"),
            P(GRP_FS, None, "tp"),
            P(GRP_FS, "tp"),
        ),
        check_vma=False,
    )
```

time: 294 us -> 181 us (0.62); the launches traced: 289 us -> 181 us
  blocking collectives: 171 us -> 0 us
  Pallas kernels: 0 us -> 164 us
  waiting for transfers between devices: 57.1 us -> 0 us
  starting transfers between devices: 15.8 us -> 0 us
  between operations: 14.3 us -> 0.83 us
  matrix products: 8.97 us -> 0.77 us
  other arithmetic: 10.9 us -> 6.47 us
    all_to_all x4 -> x0, blocking collectives: 171 us -> none  [the longest x1 83.8 us: shards(): lax.all_to_all(outbound, FS, split_axis=0, concat_axis=2, tiled=True)[0]]
    pallas_call x0 -> x1, Pallas kernels: none -> 164 us  [exchange_and_apply(): pl.pallas_call(functools.partial(kernel, sizes), out_shape=(jax.ShapeDtyp...]
    all_to_all x2 -> x0, waiting for transfers between devices: 35.1 us -> none  [the longest x1 25.2 us: exchange_in_order(): lax.all_to_all(blocks, axes[k], split_axis=k, concat_axis=k, tiled=True)]
    all_gather x2 -> x0, waiting for transfers between devices: 21.9 us -> none  [the longest x1 18.2 us: shards(): expert_rows = normalize(lax.all_gather(arrived, 'tp', axis=2, tiled=True))]
    all_to_all x2 -> x0, starting transfers between devices: 15.7 us -> none  [the longest x1 11.2 us: exchange_in_order(): lax.all_to_all(blocks, axes[k], split_axis=k, concat_axis=k, tiled=True)]
    dot_general x3 -> x0, matrix products: 8.5 us -> none  [the longest x1 4.6 us: shards(): jnp.einsum('erd,edh->erh', expert_rows, up_serve, preferred_element_type=...]
    reduce_sum x1 -> x0, other arithmetic: 3.47 us -> none  [normalize(): jnp.mean(values * values, axis=-1, keepdims=True) + epsilon]
  transfers between devices with their start and end apart: 4 -> 0, of which waited for: 4 -> 0; matrix products, arithmetic and copies ran while one was open for 3% -> 0% of each run, Pallas kernels for 0% -> 0%
where the time goes in v1:
time: 181 us
  Pallas kernels  164 us (91%)
  local copies, waits for them, and re-layouts  9.5 us (5%)
  other arithmetic  6.47 us (4%)
    pallas_call x1, Pallas kernels, exchange_and_apply(): pl.pallas_call(functools.partial(kernel, sizes), out_shape=(jax.ShapeDtyp...  164 us
    unnamed x19, local copies, waits for them, and re-layouts  5.33 us

profile of v1, /device:TPU:65, one launch (start us, length us, event | category | flops | bytes accessed | tf_op | source)
XLA Modules:
  0.0 181.1 jit_solution(13050426223187985733)
XLA Ops:
  0.6 0.0 copy-start
  0.7 0.9 copy.25
  1.5 0.1 eq.51
  1.7 1.7 reduce-window.6
  3.5 0.3 slice_reduce_fusion
  3.7 0.1 eq.47
  3.9 0.1 fusion.6
  4.0 0.2 reduce_sum.21
  4.2 0.2 copy.28
  4.4 0.3 compare_select_fusion
  4.7 0.1 copy.34
  4.8 2.1 %fusion = pred[2304,384]{1,0:T(8,128)(4,1)S(1)} fusion(s32[384,2]{0,1:T(2,128)S(1)} %copy.34), kind=kLoop, calls=%fused_computation.2 | loop fusion | flops 2654208 | bytes 887808 | tf_op jit(solution)/shard_map/reduce_or | solution.py:401
  7.0 0.0 copy-start.2
  7.0 0.0 copy-start.3
  7.0 0.0 copy-start.6
  7.0 0.8 convolution_convert_fusion
  7.8 0.4 copy-done.2
  8.2 0.3 copy-done.3
  8.5 0.3 multiply_convert_fusion
  8.8 0.9 copy-done.1
  9.7 0.1 convert_element_type.26.down_ref
  9.8 163.5 %exchange_and_apply.1 = (bf16[32,64,128]{2,1,0:T(8,128)(2,1)S(1)}, bf16[32,64,128]{2,1,0:T(8,128)(2,1)S(1)}, bf16[32,32,256]{2,1,0:T(8,128)(2,1)S(1)}, bf16[2,16,72,256]{3,2,1,0:T(8,128)(2,1)S(1)}) custom-call(bf16[32,64,128]{2,1,0:T(8,128)(2,1)S(1)} %get-tuple-element.15.gate_ref, bf16[32,64,128]{2,1,0:T(8,128)(2,1)S(1)} %get-tuple-element.14.up_ref, ...), custom_call_target="tpu_custom_call" | custom-call | tf_op jit(solution)/shard_map/exchange_and_apply/pallas_call | solution.py:333
  173.3 0.1 reshape.96
  173.5 2.7 %gather_fusion = bf16[768,256]{1,0:T(8,128)(2,1)S(1)} fusion(bf16[2304,256]{1,0:T(8,128)(2,1)S(1)} %bitcast.23, s32[1024]{0:T(1024)S(1)} %pad_clamp_fusion), kind=kCustom, calls=%fused_computation | custom fusion | bytes 789504 | tf_op jit(solution)/shard_map/gather | solution.py:407
  176.2 0.0 copy-start.5
  176.2 0.4 reshape.104
  176.6 0.3 copy-done.5
  176.9 0.1 copy.35
  177.0 1.7 multiply_reduce_fusion
  178.7 0.8 copy.44
  179.5 0.8 copy.45
  180.3 0.8 copy.46
  (9 shorter events, 0.1 us)
Async XLA Ops:
  0.6 6.3 %copy-start = (bf16[384,256]{1,0:T(8,128)(2,1)S(1)}, bf16[384,256]{1,0:T(8,128)(2,1)}, u32[]{:S(2)}) copy-start(bf16[384,256]{1,0:T(8,128)(2,1)} %param.7) | copy-start | bytes 589828
  0.6 3.5 %copy-start.4 = (s32[384,2]{0,1:T(2,128)S(1)}, s32[384,2]{0,1:T(2,128)}, u32[]{:S(2)}) copy-start(s32[384,2]{0,1:T(2,128)} %param.12) | copy-start | bytes 9220
  7.0 1.2 copy-start.2
  7.0 1.5 copy-start.3
  7.0 1.5 copy-start.6
  8.5 1.2 copy-start.1
  176.2 0.7 copy-start.5

commit v2 on v1

--- a/solution.py
+++ b/solution.py
@@ -27,13 +27,26 @@
 
 def kernel(
     sizes,
+    tok_ref,
+    route_ref,
+    mix_ref,
+    gain_ref,
+    gate_in,
+    up_in,
+    down_in,
+    gate_out,
+    up_out,
+    down_out,
+    mixture_ref,
+    wide_v,
+    wide_d,
     gate_ref,
     up_ref,
     down_ref,
+    place_v,
+    pick_hi,
+    pick_lo,
     outb_ref,
-    gate_out,
-    up_out,
-    down_out,
     ret_ref,
     swap,
     comb,
@@ -63,6 +76,7 @@
     fin_s,
     fin_r,
     out_sem,
+    in_sem,
 ):
     n_z, n_x, n_grp = sizes
     order = ring_order(n_z)
@@ -106,21 +120,69 @@
             peers.append({"fs_0": ahead(pos), "fs_1": c})
     for device in peers:
         pl.semaphore_signal(barrier, inc=1, device_id=device, device_id_type=MESH)
+
+    loads = [
+        pltpu.make_async_copy(gate_in, wide_v.at[0], in_sem.at[0]),
+        pltpu.make_async_copy(up_in, wide_v.at[1], in_sem.at[1]),
+        pltpu.make_async_copy(down_in, wide_d, in_sem.at[2]),
+    ]
+    for copy in loads:
+        copy.start()
+
+    f32, bf16 = jnp.float32, jnp.bfloat16
+    n_tok = tok_ref.shape[0]
+    experts = 2 * n_z
+    expert_ids = lax.broadcasted_iota(jnp.int32, (experts, n_tok), 0)
+    names = [jnp.where(expert_ids == route_ref[k : k + 1, :], 1.0, 0.0) for k in range(2)]
+    named = names[0] + names[1]
+    before = lax.broadcasted_iota(jnp.int32, (n_tok, n_tok), 0) < lax.broadcasted_iota(jnp.int32, (n_tok, n_tok), 1)
+    before = jnp.where(before, 1.0, 0.0).astype(bf16)
+    place = jnp.dot(named.astype(bf16), before, preferred_element_type=f32)
+    place_v[...] = jnp.where(named > 0.5, place, -1.0 - slot)
+
+    def dispatch(j, crossed):
+        distance = jnp.where(lax.rem(j, 2) == 1, (j + 1) // 2, n_z - j // 2)
+        e = lax.rem(z + distance, n_z) * 2 + jnp.where(crossed == 1, 1 - core, core)
+        slot_ids = lax.broadcasted_iota(jnp.int32, (slot, n_tok), 0).astype(f32) - CAP * crossed
+        pick = jnp.where(slot_ids == place_v[pl.ds(e, 1), :], 1.0, 0.0).astype(bf16)
+        outb_ref[crossed, j] = jnp.dot(pick, tok_ref[...], preferred_element_type=f32).astype(bf16)
+
+    def dispatch_both(j, carry):
+        dispatch(j, 1)
+        dispatch(j, 0)
+        return carry
+
+    lax.fori_loop(0, n_z, dispatch_both, 0)
     pl.semaphore_wait(barrier, len(peers))
 
     first = send(outb_ref.at[1], swap, swap_sems.at[0], swap_sems.at[1], other_core)
+
+    n_gain = gain_ref.shape[1]
+    eye = lax.broadcasted_iota(jnp.int32, (n_gain, n_gain), 0) == lax.broadcasted_iota(jnp.int32, (n_gain, n_gain), 1)
+    gain = jnp.sum(jnp.where(eye, gain_ref[...], 0.0), axis=1, keepdims=True)
+    for copy in loads:
+        copy.wait()
+
+    def cast(e, carry):
+        gate_ref[e] = (gain * wide_v[0, e]).astype(bf16)
+        up_ref[e] = (gain * wide_v[1, e]).astype(bf16)
+        down_ref[e] = wide_d[e].astype(bf16)
+        return carry
+
+    lax.fori_loop(0, experts, cast, 0)
+
     first.wait_recv()
     comb[...] = outb_ref[0] + swap[...]
     x_buf[0, 0] = outb_ref[0, 0] + swap[0]
-
-    for pos in range(1, n_z):
-        send(comb.at[pos], x_buf.at[0, pos], tok_s.at[pos], tok_r.at[pos], {"fs_0": ahead(pos)})
-
-    g_rows = pl.ds(pl.multiple_of(half * g_half, g_half), g_half)
-    d_rows = pl.ds(pl.multiple_of(half * d_half, d_half), d_half)
     gate_v[me] = gate_ref[me]
     up_v[me] = up_ref[me]
     down_v[me] = down_ref[me]
+
+    for pos in range(1, n_z):
+        send(comb.at[pos], x_buf.at[0, pos], tok_s.at[pos], tok_r.at[pos], {"fs_0": ahead(pos)})
+
+    g_rows = pl.ds(pl.multiple_of(half * g_half, g_half), g_half)
+    d_rows = pl.ds(pl.multiple_of(half * d_half, d_half), d_half)
     mate = z * 2 + 1 - core
     send(gate_ref.at[mate], gate_v.at[me], gu_s.at[0, 0, 0], gu_r.at[0, 0, 0], other_core)
     send(up_ref.at[mate], up_v.at[me], gu_s.at[0, 0, 1], gu_r.at[0, 0, 1], other_core)
@@ -184,6 +246,25 @@
             pair = pl.ds(behind(pos) * 2, 2)
             send(down_v.at[pair, d_rows], down_v.at[pair, d_rows], ydn_s.at[pos], ydn_r.at[pos], y_peer)
 
+    def build_picks():
+        chosen = []
+        for k in range(2):
+            e = route_ref[k : k + 1, :]
+            far = lax.rem(e // 2 - z + n_z, n_z)
+            pos = jnp.where(far == 0, 0, jnp.where(far <= n_z // 2, 2 * far - 1, 2 * (n_z - far)))
+            crossed = jnp.where(lax.rem(e, 2) == core, 0, 1)
+            inside = jnp.sum(names[k] * place, axis=0, keepdims=True)
+            chosen.append((crossed * (n_z * slot + CAP) + pos * slot).astype(f32) + inside)
+        chosen += [mix_ref[0:1, :], mix_ref[1:2, :]]
+        table = jnp.concatenate(chosen + [jnp.zeros((128 - len(chosen), n_tok), f32)], axis=0).T
+        step = per * slot
+        for c in range(2 * CHUNKS):
+            ids = (lax.broadcasted_iota(jnp.int32, (n_tok, step), 1) + c * step).astype(f32)
+            w = jnp.where(ids == table[:, 0:1], table[:, 2:3], 0.0) + jnp.where(ids == table[:, 1:2], table[:, 3:4], 0.0)
+            hi = w.astype(bf16)
+            pick_hi[c] = hi
+            pick_lo[c] = (w - hi.astype(f32)).astype(bf16)
+
     def hop_x(k, h):
         if h == 1:
             wait_tokens(k)
@@ -198,15 +279,16 @@
     hop_x(2, 1)
     hop_x(0, 4)
     hop_x(1, 4)
+    hop_x(2, 2)
+    build_picks()
+    hop_x(2, 3)
     hop_x(3, 1)
-    hop_x(2, 2)
+    hop_x(2, 4)
     hop_x(3, 2)
     forward_gu(0)
-    hop_x(2, 3)
     forward_gu(1)
     hop_x(3, 3)
     forward_gu(2)
-    hop_x(2, 4)
     hop_x(3, 4)
     forward_gu(3)
 
@@ -230,8 +312,7 @@
     rows = per * slot
 
     def expert_hidden(k):
-        for h in ((4,) if k < 2 else (4,)):
-            arrived(x_buf, k, h, xr)
+        arrived(x_buf, k, n_x // 2, xr)
         total = jnp.zeros((rows, 2 * gate_v.shape[2]), jnp.float32)
         square = jnp.zeros((rows, width), jnp.float32)
         for s in range(n_x):
@@ -255,7 +336,7 @@
         hop(h_buf, k, h, hs, hr)
 
     def expert_out(k):
-        arrived(h_buf, k, 4, hr)
+        arrived(h_buf, k, n_x // 2, hr)
         n_h = h_buf.shape[3]
         total = jnp.zeros((rows, width), jnp.float32)
         for s in range(n_x):
@@ -282,73 +363,98 @@
     hop_h(3, 3)
     hop_h(1, 1)
     hop_h(2, 3)
+    hop_h(3, 4)
     expert_hidden(0)
-    hop_h(3, 4)
+    hop_h(0, 1)
     hop_h(2, 4)
-    hop_h(0, 1)
     hop_h(1, 2)
     for k in range(CHUNKS):
         forward_dn(k)
     hop_h(0, 2)
-    hop_h(1, 3)
     got(down_v.at[mate], dn_r.at[0, 0])
     for pos in range(1, n_z):
         got(down_v.at[pl.ds(behind(pos) * 2, 2), o_d_rows], ydn_r.at[pos])
     outs[2].start()
     expert_out(3)
     send_out(3)
+    hop_h(1, 3)
     hop_h(0, 3)
-    hop_h(1, 4)
     expert_out(2)
     send_out(2)
+    hop_h(1, 4)
     hop_h(0, 4)
     expert_out(1)
     send_out(1)
     expert_out(0)
     send_out(0)
 
-    for k in reversed(range(CHUNKS)):
-        part = pl.ds(k * per, per)
+    def mixed(c, k):
+        data = ret_ref[c, k * per : (k + 1) * per].reshape(rows, width)
+        part = jnp.dot(pick_hi[c * CHUNKS + k], data, preferred_element_type=f32)
+        return part + jnp.dot(pick_lo[c * CHUNKS + k], data, preferred_element_type=f32)
+
+    total = jnp.zeros((n_tok, width), f32)
+    backs = (3, 2, 1, 0)
+    for n, k in enumerate(backs):
         for pos in range(k * per, (k + 1) * per):
             if pos:
                 got(ret_ref.at[0, pos], ret_r.at[pos])
+        part = pl.ds(k * per, per)
         send(ret_ref.at[0, part], ret_ref.at[1, part], fin_s.at[k], fin_r.at[k], other_core)
-    for k in reversed(range(CHUNKS)):
-        got(ret_ref.at[1, pl.ds(k * per, per)], fin_r.at[k])
+        total = total + mixed(0, k)
+        if n:
+            got(ret_ref.at[1, pl.ds(backs[n - 1] * per, per)], fin_r.at[backs[n - 1]])
+            total = total + mixed(1, backs[n - 1])
+    got(ret_ref.at[1, pl.ds(backs[-1] * per, per)], fin_r.at[backs[-1]])
+    total = total + mixed(1, backs[-1])
+    mixture_ref[...] = total.astype(bf16)
     for copy in outs:
         copy.wait()
     for copy in sends:
         copy.wait_send()
 
 
-def exchange_and_apply(gate_low, up_low, down_low, outb, sizes):
+def exchange_and_apply(tokens, routes, mix, gain, gate, up, down, sizes):
     n_z, n_x, n_grp = sizes
-    bf16 = jnp.bfloat16
-    _, _, slot, width = outb.shape
-    n_h = gate_low.shape[2]
+    f32, bf16 = jnp.float32, jnp.bfloat16
+    n_tok, width = tokens.shape
+    slot = 2 * CAP
+    n_h = gate.shape[2]
+    experts = gate.shape[0]
     dma = pltpu.SemaphoreType.DMA
     hops = n_x // 2
     vmem = pl.BlockSpec(memory_space=pltpu.VMEM)
     hbm = pl.BlockSpec(memory_space=pl.ANY)
+    picks = (2 * CHUNKS, n_tok, n_z // CHUNKS * slot)
     return pl.pallas_call(
         functools.partial(kernel, sizes),
         out_shape=(
-            jax.ShapeDtypeStruct(gate_low.shape, bf16),
-            jax.ShapeDtypeStruct(up_low.shape, bf16),
-            jax.ShapeDtypeStruct(down_low.shape, bf16),
-            jax.ShapeDtypeStruct(outb.shape, bf16),
+            jax.ShapeDtypeStruct(gate.shape, bf16),
+            jax.ShapeDtypeStruct(up.shape, bf16),
+            jax.ShapeDtypeStruct(down.shape, bf16),
+            jax.ShapeDtypeStruct(tokens.shape, bf16),
         ),
-        in_specs=[vmem] * 4,
+        in_specs=[vmem] * 4 + [hbm] * 3,
         out_specs=(hbm, hbm, hbm, vmem),
         scratch_shapes=[
-            pltpu.VMEM(outb.shape[1:], bf16),
-            pltpu.VMEM(outb.shape[1:], bf16),
+            pltpu.VMEM((2,) + gate.shape, f32),
+            pltpu.VMEM(down.shape, f32),
+            pltpu.VMEM(gate.shape, bf16),
+            pltpu.VMEM(up.shape, bf16),
+            pltpu.VMEM(down.shape, bf16),
+            pltpu.VMEM((experts, n_tok), f32),
+            pltpu.VMEM(picks, bf16),
+            pltpu.VMEM(picks, bf16),
+            pltpu.VMEM((2, n_z, slot, width), bf16),
+            pltpu.VMEM((2, n_z, slot, width), bf16),
+            pltpu.VMEM((n_z, slot, width), bf16),
+            pltpu.VMEM((n_z, slot, width), bf16),
             pltpu.VMEM((n_x, n_z, slot, width), bf16),
             pltpu.VMEM((n_x, n_z, slot, n_h), bf16),
-            pltpu.VMEM(outb.shape[1:], bf16),
-            pltpu.VMEM(gate_low.shape, bf16),
-            pltpu.VMEM(up_low.shape, bf16),
-            pltpu.VMEM(down_low.shape, bf16),
+            pltpu.VMEM((n_z, slot, width), bf16),
+            pltpu.VMEM(gate.shape, bf16),
+            pltpu.VMEM(up.shape, bf16),
+            pltpu.VMEM(down.shape, bf16),
             dma((2,)),
             dma((n_z,)),
             dma((n_z,)),
@@ -369,44 +475,19 @@
             dma((CHUNKS,)),
             dma((CHUNKS,)),
             dma((3,)),
+            dma((3,)),
         ],
         compiler_params=pltpu.CompilerParams(
             collective_id=0, has_side_effects=True, vmem_limit_bytes=40 * 1024 * 1024
         ),
         name="exchange_and_apply",
-    )(gate_low, up_low, down_low, outb)
+    )(tokens, routes, mix, gain, gate, up, down)
 
 
 def shards(tokens, norm_gain, gate_weight, up_weight, down_weight, routes, route_weights):
-    experts = gate_weight.shape[0]
-    n_z = lax.axis_size("fs_0")
-    n_x = lax.axis_size("tp")
-    n_grp = lax.axis_size("grp")
-    tok_rows, width = tokens.shape
-    gate_low = (norm_gain[None, :, None] * gate_weight).astype(jnp.bfloat16)
-    up_low = (norm_gain[None, :, None] * up_weight).astype(jnp.bfloat16)
-    down_low = down_weight.astype(jnp.bfloat16)
-
-    flat_routes = routes.reshape(-1)
-    expert_ids = lax.iota(jnp.int32, experts)
-    onehot = (flat_routes[:, None] == expert_ids[None, :]).astype(jnp.int32)
-    position = jnp.sum((jnp.cumsum(onehot, axis=0) - 1) * onehot, axis=1)
-    order = ring_order(n_z)
-    distance = lax.rem(flat_routes // 2 - lax.axis_index("fs_0") + n_z, n_z)
-    pos = jnp.where(distance == 0, 0, jnp.where(distance <= n_z // 2, 2 * distance - 1, 2 * (n_z - distance)))
-    crossed = jnp.abs(lax.rem(flat_routes, 2) - lax.axis_index("fs_1"))
-    slots = 2 * CAP
-    slot_index = (crossed * (n_z * slots + CAP) + pos * slots + position).reshape(tok_rows, 2)
-    slot_ids = lax.iota(jnp.int32, 2 * n_z * slots)
-    select = jnp.any(slot_ids[:, None, None] == slot_index[None, :, :], axis=2).astype(jnp.bfloat16)
-    outbound = jnp.dot(select, tokens, preferred_element_type=jnp.float32).astype(jnp.bfloat16)
-    outbound = outbound.reshape(2, n_z, slots, width)
-    gate_serve, up_serve, down_serve, back = exchange_and_apply(
-        gate_low, up_low, down_low, outbound, (n_z, n_x, n_grp)
-    )
-    picked = back.reshape(2 * n_z * slots, width)[slot_index]
-    mixture = jnp.sum(route_weights[:, :, None] * picked.astype(jnp.float32), axis=1).astype(
-        jnp.bfloat16
+    sizes = (lax.axis_size("fs_0"), lax.axis_size("tp"), lax.axis_size("grp"))
+    gate_serve, up_serve, down_serve, mixture = exchange_and_apply(
+        tokens, routes.T, route_weights.T, norm_gain[None, :], gate_weight, up_weight, down_weight, sizes
     )
     return (
         gate_serve.reshape(1, -1, gate_serve.shape[2]),

time: 181 us -> 177 us (0.978)
  other arithmetic: 6.47 us -> 0 us
  Pallas kernels: 164 us -> 167 us
    pallas_call x1, Pallas kernels: 164 us -> 167 us  [exchange_and_apply(): pl.pallas_call(functools.partial(kernel, sizes), out_shape=(jax.ShapeDtyp...]
    unnamed x19 -> x18, local copies, waits for them, and re-layouts: 5.33 us -> 9.01 us
    gather x1 -> x0, local copies, waits for them, and re-layouts: 2.66 us -> none  [shards(): picked = back.reshape(2 * n_z * slots, width)[slot_index]]
    reduce_or x1 -> x0, other arithmetic: 2.15 us -> none  [shards(): jnp.any(slot_ids[:, None, None] == slot_index[None, :, :], axis=2)]
    reduce_sum x2 -> x0, other arithmetic: 1.82 us -> none  [the longest x1 1.72 us: shards(): jnp.sum(route_weights[:, :, None] * picked.astype(jnp.float32), axis=1)]
where the time goes in v2:
time: 177 us
  Pallas kernels  167 us (94%)
  local copies, waits for them, and re-layouts  9.01 us (5%)
    pallas_call x1, Pallas kernels, exchange_and_apply(): pl.pallas_call(functools.partial(kernel, sizes), out_shape=(jax.ShapeDtyp...  167 us
    unnamed x18, local copies, waits for them, and re-layouts  9.01 us

profile of v2, /device:TPU:65, one launch (start us, length us, event | category | flops | bytes accessed | tf_op | source)
XLA Modules:
  0.0 177.0 jit_solution(5149428902191134627)
XLA Ops:
  0.6 0.0 copy-start.4
  0.6 0.0 copy-start.6
  0.7 0.7 copy-done.4
  1.3 0.0 copy-done.6
  1.3 0.0 copy-start
  1.3 1.2 copy-done
  2.5 0.0 copy-start.1
  2.5 1.2 copy-done.1
  3.8 0.0 copy-start.2
  3.8 1.2 copy-done.2
  5.0 0.0 copy-start.3
  5.0 0.9 copy-done.3
  5.9 0.0 copy-start.5
  5.9 0.7 copy-done.5
  6.6 167.3 %exchange_and_apply.1 = (bf16[32,64,128]{2,1,0:T(8,128)(2,1)S(1)}, bf16[32,64,128]{2,1,0:T(8,128)(2,1)S(1)}, bf16[32,32,256]{2,1,0:T(8,128)(2,1)S(1)}, bf16[384,256]{1,0:T(8,128)(2,1)S(1)}) custom-call(bf16[384,256]{1,0:T(8,128)(2,1)S(1)} %copy-done.3, s32[2,384]{1,0:T(2,128)S(1)} %bitcast.9, f32[2,384]{1,0:T(2,128)S(1)} %bitcast.10, f32[1,64]{1,0:T(1,128)S(1)} %bitcast.11, ...), custom_call_target="tpu_custom_call" | custom-call | tf_op jit(solution)/shard_map/exchange_and_apply/pallas_call | solution.py:429
  173.9 0.8 copy.15
  174.7 0.8 copy.16
  175.5 0.8 copy.17
  176.3 0.7 copy.18
Async XLA Ops:
  0.6 0.7 copy-start.4
  0.6 0.7 copy-start.6
  1.3 1.2 copy-start
  2.5 1.2 copy-start.1
  3.8 1.2 copy-start.2
  5.0 0.9 copy-start.3
  5.9 0.7 copy-start.5

commit v3 on v2

--- a/solution.py
+++ b/solution.py
@@ -13,7 +13,7 @@
 GRP_FS = ("grp", "fs_0", "fs_1")
 MESH = pl.DeviceIdType.MESH
 EPSILON = 1e-06
-CHUNKS = 4
+CHUNKS = 8
 
 
 def ring_order(n):
@@ -77,6 +77,11 @@
     fin_r,
     out_sem,
     in_sem,
+    stage_x,
+    stage_gu,
+    stage_dn,
+    stage_s,
+    stage_r,
 ):
     n_z, n_x, n_grp = sizes
     order = ring_order(n_z)
@@ -94,7 +99,7 @@
     other_core = {"fs_1": 1 - core}
     right = {"tp": lax.rem(x + 1, n_x)}
     left = {"tp": lax.rem(x + n_x - 1, n_x)}
-    sends = []
+    sends, late_sends = [], []
 
     def ahead(pos):
         return lax.rem(z + order[pos], n_z)
@@ -178,8 +183,41 @@
     up_v[me] = up_ref[me]
     down_v[me] = down_ref[me]
 
-    for pos in range(1, n_z):
+    opposite = n_z - 1
+    leg = {"fs_0": lax.rem(z + n_z - n_z // 4, n_z)}
+    origin = lax.rem(z + n_z // 4, n_z) * 2 + 1
+    relays = core == 1
+
+    def leg_dest(c):
+        return {"fs_0": lax.rem(z + n_z - n_z // 4, n_z), "fs_1": c}
+
+    def first_leg(n, src, stage):
+        remote(src, stage, stage_s.at[n, 0], stage_r.at[n], leg).start()
+
+    def second_leg(n, stage, dst, recv_sem, device):
+        got(stage, stage_r.at[n])
+        remote(stage, dst, stage_s.at[n, 1], recv_sem, device).start()
+
+    def got(ref, sem):
+        pltpu.make_async_copy(ref, ref, sem).wait()
+
+    @pl.when(relays)
+    def _():
+        first_leg(0, comb.at[opposite], stage_x.at[0])
+
+    for pos in range(1, n_z - 1):
         send(comb.at[pos], x_buf.at[0, pos], tok_s.at[pos], tok_r.at[pos], {"fs_0": ahead(pos)})
+
+    @pl.when(jnp.logical_not(relays))
+    def _():
+        remote(
+            comb.at[opposite], x_buf.at[0, opposite], tok_s.at[opposite], tok_r.at[opposite], {"fs_0": ahead(opposite)}
+        ).start()
+
+    def relay_tokens():
+        @pl.when(relays)
+        def _():
+            second_leg(0, stage_x.at[0], x_buf.at[0, opposite], tok_r.at[opposite], leg)
 
     g_rows = pl.ds(pl.multiple_of(half * g_half, g_half), g_half)
     d_rows = pl.ds(pl.multiple_of(half * d_half, d_half), d_half)
@@ -187,22 +225,72 @@
     send(gate_ref.at[mate], gate_v.at[me], gu_s.at[0, 0, 0], gu_r.at[0, 0, 0], other_core)
     send(up_ref.at[mate], up_v.at[me], gu_s.at[0, 0, 1], gu_r.at[0, 0, 1], other_core)
     send(down_ref.at[mate], down_v.at[me], dn_s.at[0, 0], dn_r.at[0, 0], other_core)
-    for pos in range(1, n_z):
-        for c in range(2):
-            cc = lax.rem(core + c, 2)
-            e = ahead(pos) * 2 + cc
-            device = {"fs_0": ahead(pos), "fs_1": cc}
-            send(gate_ref.at[e, g_rows], gate_v.at[me, g_rows], gu_s.at[pos, c, 0], gu_r.at[pos, c, 0], device)
-            send(up_ref.at[e, g_rows], up_v.at[me, g_rows], gu_s.at[pos, c, 1], gu_r.at[pos, c, 1], device)
-    for pos in range(1, n_z):
-        for c in range(2):
-            cc = lax.rem(core + c, 2)
-            e = ahead(pos) * 2 + cc
-            device = {"fs_0": ahead(pos), "fs_1": cc}
-            send(down_ref.at[e, d_rows], down_v.at[me, d_rows], dn_s.at[pos, c], dn_r.at[pos, c], device)
-
-    def got(ref, sem):
-        pltpu.make_async_copy(ref, ref, sem).wait()
+    def gate_up_copies(pos, c):
+        cc = lax.rem(core + c, 2)
+        e = ahead(pos) * 2 + cc
+        device = {"fs_0": ahead(pos), "fs_1": cc}
+        return (
+            remote(gate_ref.at[e, g_rows], gate_v.at[me, g_rows], gu_s.at[pos, c, 0], gu_r.at[pos, c, 0], device),
+            remote(up_ref.at[e, g_rows], up_v.at[me, g_rows], gu_s.at[pos, c, 1], gu_r.at[pos, c, 1], device),
+        )
+
+    def down_copies(pos, c):
+        cc = lax.rem(core + c, 2)
+        e = ahead(pos) * 2 + cc
+        device = {"fs_0": ahead(pos), "fs_1": cc}
+        return (remote(down_ref.at[e, d_rows], down_v.at[me, d_rows], dn_s.at[pos, c], dn_r.at[pos, c], device),)
+
+    def send_weights(copies_of):
+        for pos in range(1, n_z - 1):
+            for c in range(2):
+                for copy in copies_of(pos, c):
+                    copy.start()
+                    sends.append(copy)
+
+        @pl.when(jnp.logical_not(relays))
+        def _():
+            for c in range(2):
+                for copy in copies_of(opposite, c):
+                    copy.start()
+
+    def send_gate_up():
+        @pl.when(relays)
+        def _():
+            for c in range(2):
+                e = ahead(opposite) * 2 + c
+                first_leg(1 + 2 * c, gate_ref.at[e, g_rows], stage_gu.at[c, 0])
+                first_leg(2 + 2 * c, up_ref.at[e, g_rows], stage_gu.at[c, 1])
+
+        send_weights(gate_up_copies)
+
+    def relay_gate_up():
+        @pl.when(relays)
+        def _():
+            for c in range(2):
+                n = 1 - c
+                second_leg(
+                    1 + 2 * c, stage_gu.at[c, 0], gate_v.at[origin, g_rows], gu_r.at[opposite, n, 0], leg_dest(c)
+                )
+                second_leg(2 + 2 * c, stage_gu.at[c, 1], up_v.at[origin, g_rows], gu_r.at[opposite, n, 1], leg_dest(c))
+
+    def send_down():
+        @pl.when(relays)
+        def _():
+            for c in range(2):
+                first_leg(5 + c, down_ref.at[ahead(opposite) * 2 + c, d_rows], stage_dn.at[c])
+
+        send_weights(down_copies)
+
+    def relay_down():
+        @pl.when(relays)
+        def _():
+            for c in range(2):
+                second_leg(5 + c, stage_dn.at[c], down_v.at[origin, d_rows], dn_r.at[opposite, 1 - c], leg_dest(c))
+
+    def relay_back():
+        @pl.when(relays)
+        def _():
+            second_leg(7, stage_x.at[1], ret_ref.at[0, opposite], ret_r.at[opposite], leg)
 
     def wait_tokens(k):
         for pos in range(k * per, (k + 1) * per):
@@ -270,27 +358,25 @@
             wait_tokens(k)
         hop(x_buf, k, h, xs, xr)
 
-    hop_x(0, 1)
-    hop_x(1, 1)
-    hop_x(0, 2)
-    hop_x(1, 2)
-    hop_x(0, 3)
-    hop_x(1, 3)
-    hop_x(2, 1)
-    hop_x(0, 4)
-    hop_x(1, 4)
-    hop_x(2, 2)
-    build_picks()
-    hop_x(2, 3)
-    hop_x(3, 1)
-    hop_x(2, 4)
-    hop_x(3, 2)
-    forward_gu(0)
-    forward_gu(1)
-    hop_x(3, 3)
-    forward_gu(2)
-    hop_x(3, 4)
-    forward_gu(3)
+    top = n_x // 2
+    begins = (0, 0, 1, 2, 2, 3, 4, 5)
+    gate_up_rounds = {6: (0, 1, 2), 7: (3, 4, 5), 8: (6, 7)}
+    for r in range(begins[-1] + top):
+        for k in range(CHUNKS):
+            if 0 <= r - begins[k] < top:
+                hop_x(k, r - begins[k] + 1)
+        if r == 1:
+            relay_tokens()
+            send_gate_up()
+        if r == 2:
+            build_picks()
+        if r == 5:
+            relay_gate_up()
+            send_down()
+        for k in gate_up_rounds.get(r, ()):
+            forward_gu(k)
+
+    relay_down()
 
     o_g_rows = pl.ds(pl.multiple_of((1 - half) * g_half, g_half), g_half)
     o_d_rows = pl.ds(pl.multiple_of((1 - half) * d_half, d_half), d_half)
@@ -307,6 +393,12 @@
     ]
     outs[0].start()
     outs[1].start()
+
+    def wait_down():
+        got(down_v.at[mate], dn_r.at[0, 0])
+        for pos in range(1, n_z):
+            got(down_v.at[pl.ds(behind(pos) * 2, 2), o_d_rows], ydn_r.at[pos])
+        outs[2].start()
 
     f_src = 2 * n_z // n_x
     rows = per * slot
@@ -349,44 +441,59 @@
     def send_out(k):
         for pos in reversed(range(k * per, (k + 1) * per)):
             if pos:
-                send(o_buf.at[pos], ret_ref.at[0, pos], ret_s.at[pos], ret_r.at[pos], {"fs_0": behind(pos)})
+                copy = remote(o_buf.at[pos], ret_ref.at[0, pos], ret_s.at[pos], ret_r.at[pos], {"fs_0": behind(pos)})
+                if pos < opposite:
+                    copy.start()
+                    late_sends.append(copy)
+                    continue
+
+                @pl.when(relays)
+                def _():
+                    first_leg(7, o_buf.at[pos], stage_x.at[1])
+
+                @pl.when(jnp.logical_not(relays))
+                def _():
+                    copy.start()
             else:
                 ret_ref[0, 0] = o_buf[0]
 
-    expert_hidden(3)
-    hop_h(3, 1)
-    expert_hidden(2)
-    hop_h(2, 1)
-    hop_h(3, 2)
-    expert_hidden(1)
-    hop_h(2, 2)
-    hop_h(3, 3)
-    hop_h(1, 1)
-    hop_h(2, 3)
-    hop_h(3, 4)
-    expert_hidden(0)
-    hop_h(0, 1)
-    hop_h(2, 4)
-    hop_h(1, 2)
-    for k in range(CHUNKS):
+    near, far = tuple(range(CHUNKS // 2 - 1, -1, -1)), tuple(range(CHUNKS - 1, CHUNKS // 2 - 1, -1))
+
+    def hops(chunks, h):
+        for k in chunks:
+            if h == 1:
+                expert_hidden(k)
+            hop_h(k, h)
+
+    def finish(chunks):
+        for k in chunks:
+            expert_out(k)
+            send_out(k)
+
+    hops(far, 1)
+    for k in range(0, 5):
         forward_dn(k)
-    hop_h(0, 2)
-    got(down_v.at[mate], dn_r.at[0, 0])
-    for pos in range(1, n_z):
-        got(down_v.at[pl.ds(behind(pos) * 2, 2), o_d_rows], ydn_r.at[pos])
-    outs[2].start()
-    expert_out(3)
-    send_out(3)
-    hop_h(1, 3)
-    hop_h(0, 3)
-    expert_out(2)
-    send_out(2)
-    hop_h(1, 4)
-    hop_h(0, 4)
-    expert_out(1)
-    send_out(1)
-    expert_out(0)
-    send_out(0)
+    hops(far, 2)
+    forward_dn(5)
+    hops(near, 1)
+    hops(far, 3)
+    forward_dn(6)
+    hops(near, 2)
+    forward_dn(7)
+    hops(far, 4)
+    wait_down()
+    finish(far[:2])
+    hops(near, 3)
+    finish(far[2:])
+    relay_back()
+    hops(near, 4)
+    finish(near)
+    for copy in sends:
+        copy.wait_send()
+    sends.clear()
+    outs[0].wait()
+    outs[1].wait()
+    outs[2].wait()
 
     def mixed(c, k):
         data = ret_ref[c, k * per : (k + 1) * per].reshape(rows, width)
@@ -394,13 +501,15 @@
         return part + jnp.dot(pick_lo[c * CHUNKS + k], data, preferred_element_type=f32)
 
     total = jnp.zeros((n_tok, width), f32)
-    backs = (3, 2, 1, 0)
+    backs = tuple(reversed(range(CHUNKS)))
     for n, k in enumerate(backs):
         for pos in range(k * per, (k + 1) * per):
             if pos:
                 got(ret_ref.at[0, pos], ret_r.at[pos])
         part = pl.ds(k * per, per)
-        send(ret_ref.at[0, part], ret_ref.at[1, part], fin_s.at[k], fin_r.at[k], other_core)
+        copy = remote(ret_ref.at[0, part], ret_ref.at[1, part], fin_s.at[k], fin_r.at[k], other_core)
+        copy.start()
+        late_sends.append(copy)
         total = total + mixed(0, k)
         if n:
             got(ret_ref.at[1, pl.ds(backs[n - 1] * per, per)], fin_r.at[backs[n - 1]])
@@ -408,10 +517,27 @@
     got(ret_ref.at[1, pl.ds(backs[-1] * per, per)], fin_r.at[backs[-1]])
     total = total + mixed(1, backs[-1])
     mixture_ref[...] = total.astype(bf16)
-    for copy in outs:
-        copy.wait()
-    for copy in sends:
+    for copy in late_sends:
         copy.wait_send()
+
+    @pl.when(relays)
+    def _():
+        for n in range(2):
+            got(stage_x.at[0], stage_s.at[0, n])
+            got(stage_x.at[1], stage_s.at[7, n])
+            for c in range(2):
+                got(stage_gu.at[c, 0], stage_s.at[1 + 2 * c, n])
+                got(stage_gu.at[c, 1], stage_s.at[2 + 2 * c, n])
+                got(stage_dn.at[c], stage_s.at[5 + c, n])
+
+    @pl.when(jnp.logical_not(relays))
+    def _():
+        got(comb.at[opposite], tok_s.at[opposite])
+        got(o_buf.at[opposite], ret_s.at[opposite])
+        for c in range(2):
+            got(stage_gu.at[c, 0], gu_s.at[opposite, c, 0])
+            got(stage_gu.at[c, 1], gu_s.at[opposite, c, 1])
+            got(stage_dn.at[c], dn_s.at[opposite, c])
 
 
 def exchange_and_apply(tokens, routes, mix, gain, gate, up, down, sizes):
@@ -476,9 +602,14 @@
             dma((CHUNKS,)),
             dma((3,)),
             dma((3,)),
+            pltpu.VMEM((2, slot, width), bf16),
+            pltpu.VMEM((2, 2, gate.shape[1] // 2, n_h), bf16),
+            pltpu.VMEM((2, down.shape[1] // 2, width), bf16),
+            dma((8, 2)),
+            dma((8,)),
         ],
         compiler_params=pltpu.CompilerParams(
-            collective_id=0, has_side_effects=True, vmem_limit_bytes=40 * 1024 * 1024
+            collective_id=0, has_side_effects=True, vmem_limit_bytes=67043328
         ),
         name="exchange_and_apply",
     )(tokens, routes, mix, gain, gate, up, down)

time: 177 us -> 174 us (0.983)
  local copies, waits for them, and re-layouts: 9.01 us -> 4.95 us
    unnamed x18 -> x10, local copies, waits for them, and re-layouts: 9.01 us -> 4.95 us
where the time goes in v3:
time: 174 us
  Pallas kernels  168 us (97%)
  local copies, waits for them, and re-layouts  4.95 us (3%)
    pallas_call x1, Pallas kernels, exchange_and_apply(): pl.pallas_call(functools.partial(kernel, sizes), out_shape=(jax.ShapeDtyp...  168 us
    unnamed x10, local copies, waits for them, and re-layouts  4.95 us

profile of v3, /device:TPU:65, one launch (start us, length us, event | category | flops | bytes accessed | tf_op | source)
XLA Modules:
  0.0 174.1 jit_solution(5756477401254690559)
XLA Ops:
  0.6 168.5 %exchange_and_apply.1 = (bf16[32,64,128]{2,1,0:T(8,128)(2,1)}, bf16[32,64,128]{2,1,0:T(8,128)(2,1)}, bf16[32,32,256]{2,1,0:T(8,128)(2,1)}, bf16[384,256]{1,0:T(8,128)(2,1)}) custom-call(bf16[384,256]{1,0:T(8,128)(2,1)} %tok_ref.1, s32[2,384]{1,0:T(2,128)} %bitcast.9, f32[2,384]{1,0:T(2,128)} %bitcast.10, f32[1,64]{1,0:T(1,128)} %bitcast.11, ...), custom_call_target="tpu_custom_call" | custom-call | tf_op jit(solution)/shard_map/exchange_and_apply/pallas_call | solution.py:555
  169.1 0.0 copy-start.1
  169.1 1.9 %copy.15 = bf16[1,2048,128]{2,1,0:T(8,128)(2,1)} copy(bf16[1,2048,128]{2,1,0:T(8,128)(2,1)} %bitcast.8) | data formatting | bytes 1048576
  171.1 0.0 copy-done.1
  171.1 0.0 copy-start
  171.1 0.8 copy.16
  171.9 0.4 copy-done
  172.3 0.0 copy-start.2
  172.3 0.8 copy.17
  173.1 0.3 copy-done.2
  173.4 0.7 copy.18
Async XLA Ops:
  169.1 1.9 %copy-start.1 = (bf16[32,64,128]{2,1,0:T(8,128)(2,1)S(1)}, bf16[32,64,128]{2,1,0:T(8,128)(2,1)}, u32[]{:S(2)}) copy-start(bf16[32,64,128]{2,1,0:T(8,128)(2,1)} %get-tuple-element.9) | copy-start | bytes 1572868
  171.1 1.2 copy-start
  172.3 1.1 copy-start.2

commit v4 on v3

--- a/solution.py
+++ b/solution.py
@@ -99,7 +99,6 @@
     other_core = {"fs_1": 1 - core}
     right = {"tp": lax.rem(x + 1, n_x)}
     left = {"tp": lax.rem(x + n_x - 1, n_x)}
-    sends, late_sends = [], []
 
     def ahead(pos):
         return lax.rem(z + order[pos], n_z)
@@ -115,7 +114,6 @@
     def send(*args):
         copy = remote(*args)
         copy.start()
-        sends.append(copy)
         return copy
 
     barrier = pltpu.get_barrier_semaphore()
@@ -206,12 +204,12 @@
         first_leg(0, comb.at[opposite], stage_x.at[0])
 
     for pos in range(1, n_z - 1):
-        send(comb.at[pos], x_buf.at[0, pos], tok_s.at[pos], tok_r.at[pos], {"fs_0": ahead(pos)})
+        send(comb.at[pos], x_buf.at[0, pos], tok_s.at[0], tok_r.at[pos], {"fs_0": ahead(pos)})
 
     @pl.when(jnp.logical_not(relays))
     def _():
         remote(
-            comb.at[opposite], x_buf.at[0, opposite], tok_s.at[opposite], tok_r.at[opposite], {"fs_0": ahead(opposite)}
+            comb.at[opposite], x_buf.at[0, opposite], tok_s.at[0], tok_r.at[opposite], {"fs_0": ahead(opposite)}
         ).start()
 
     def relay_tokens():
@@ -222,30 +220,29 @@
     g_rows = pl.ds(pl.multiple_of(half * g_half, g_half), g_half)
     d_rows = pl.ds(pl.multiple_of(half * d_half, d_half), d_half)
     mate = z * 2 + 1 - core
-    send(gate_ref.at[mate], gate_v.at[me], gu_s.at[0, 0, 0], gu_r.at[0, 0, 0], other_core)
-    send(up_ref.at[mate], up_v.at[me], gu_s.at[0, 0, 1], gu_r.at[0, 0, 1], other_core)
-    send(down_ref.at[mate], down_v.at[me], dn_s.at[0, 0], dn_r.at[0, 0], other_core)
+    send(gate_ref.at[mate], gate_v.at[me], gu_s.at[0], gu_r.at[0, 0, 0], other_core)
+    send(up_ref.at[mate], up_v.at[me], gu_s.at[0], gu_r.at[0, 0, 1], other_core)
+    send(down_ref.at[mate], down_v.at[me], dn_s.at[0], dn_r.at[0, 0], other_core)
     def gate_up_copies(pos, c):
         cc = lax.rem(core + c, 2)
         e = ahead(pos) * 2 + cc
         device = {"fs_0": ahead(pos), "fs_1": cc}
         return (
-            remote(gate_ref.at[e, g_rows], gate_v.at[me, g_rows], gu_s.at[pos, c, 0], gu_r.at[pos, c, 0], device),
-            remote(up_ref.at[e, g_rows], up_v.at[me, g_rows], gu_s.at[pos, c, 1], gu_r.at[pos, c, 1], device),
+            remote(gate_ref.at[e, g_rows], gate_v.at[me, g_rows], gu_s.at[0], gu_r.at[pos, c, 0], device),
+            remote(up_ref.at[e, g_rows], up_v.at[me, g_rows], gu_s.at[0], gu_r.at[pos, c, 1], device),
         )
 
     def down_copies(pos, c):
         cc = lax.rem(core + c, 2)
         e = ahead(pos) * 2 + cc
         device = {"fs_0": ahead(pos), "fs_1": cc}
-        return (remote(down_ref.at[e, d_rows], down_v.at[me, d_rows], dn_s.at[pos, c], dn_r.at[pos, c], device),)
+        return (remote(down_ref.at[e, d_rows], down_v.at[me, d_rows], dn_s.at[0], dn_r.at[pos, c], device),)
 
     def send_weights(copies_of):
         for pos in range(1, n_z - 1):
             for c in range(2):
                 for copy in copies_of(pos, c):
                     copy.start()
-                    sends.append(copy)
 
         @pl.when(jnp.logical_not(relays))
         def _():
@@ -304,9 +301,9 @@
         if h > 1:
             arrived(buf, k, h - 1, r_sems)
         rows = first_half if h == last else whole
-        send(buf.at[h - 1, rows], buf.at[h, rows], s_sems.at[k, h - 1, 0], r_sems.at[k, h - 1, 0], right)
+        send(buf.at[h - 1, rows], buf.at[h, rows], s_sems.at[0], r_sems.at[k, h - 1, 0], right)
         rows = second_half if h == last else whole
-        send(buf.at[(n_x - h + 1) % n_x, rows], buf.at[n_x - h, rows], s_sems.at[k, h - 1, 1], r_sems.at[k, h - 1, 1], left)
+        send(buf.at[(n_x - h + 1) % n_x, rows], buf.at[n_x - h, rows], s_sems.at[0], r_sems.at[k, h - 1, 1], left)
 
     def arrived(buf, k, h, r_sems):
         last = n_x // 2
@@ -323,8 +320,8 @@
                 got(gate_v.at[s, g_rows], gu_r.at[pos, c, 0])
                 got(up_v.at[s, g_rows], gu_r.at[pos, c, 1])
             pair = pl.ds(behind(pos) * 2, 2)
-            send(gate_v.at[pair, g_rows], gate_v.at[pair, g_rows], ygu_s.at[pos, 0], ygu_r.at[pos, 0], y_peer)
-            send(up_v.at[pair, g_rows], up_v.at[pair, g_rows], ygu_s.at[pos, 1], ygu_r.at[pos, 1], y_peer)
+            send(gate_v.at[pair, g_rows], gate_v.at[pair, g_rows], ygu_s.at[0], ygu_r.at[pos, 0], y_peer)
+            send(up_v.at[pair, g_rows], up_v.at[pair, g_rows], ygu_s.at[0], ygu_r.at[pos, 1], y_peer)
 
     def forward_dn(k):
         for pos in range(max(1, k * per), (k + 1) * per):
@@ -332,7 +329,7 @@
                 cc = lax.rem(core + c, 2)
                 got(down_v.at[behind(pos) * 2 + cc, d_rows], dn_r.at[pos, c])
             pair = pl.ds(behind(pos) * 2, 2)
-            send(down_v.at[pair, d_rows], down_v.at[pair, d_rows], ydn_s.at[pos], ydn_r.at[pos], y_peer)
+            send(down_v.at[pair, d_rows], down_v.at[pair, d_rows], ydn_s.at[0], ydn_r.at[pos], y_peer)
 
     def build_picks():
         chosen = []
@@ -360,7 +357,7 @@
 
     top = n_x // 2
     begins = (0, 0, 1, 2, 2, 3, 4, 5)
-    gate_up_rounds = {6: (0, 1, 2), 7: (3, 4, 5), 8: (6, 7)}
+    gate_up_rounds = {6: (0, 1, 2), 7: (3, 4, 5, 6), 8: (7,)}
     for r in range(begins[-1] + top):
         for k in range(CHUNKS):
             if 0 <= r - begins[k] < top:
@@ -441,10 +438,9 @@
     def send_out(k):
         for pos in reversed(range(k * per, (k + 1) * per)):
             if pos:
-                copy = remote(o_buf.at[pos], ret_ref.at[0, pos], ret_s.at[pos], ret_r.at[pos], {"fs_0": behind(pos)})
+                copy = remote(o_buf.at[pos], ret_ref.at[0, pos], ret_s.at[0], ret_r.at[pos], {"fs_0": behind(pos)})
                 if pos < opposite:
                     copy.start()
-                    late_sends.append(copy)
                     continue
 
                 @pl.when(relays)
@@ -478,9 +474,9 @@
     hops(near, 1)
     hops(far, 3)
     forward_dn(6)
-    hops(near, 2)
     forward_dn(7)
     hops(far, 4)
+    hops(near, 2)
     wait_down()
     finish(far[:2])
     hops(near, 3)
@@ -488,9 +484,25 @@
     relay_back()
     hops(near, 4)
     finish(near)
-    for copy in sends:
-        copy.wait_send()
-    sends.clear()
+    first.wait_send()
+    serving = n_z * 2
+    got(x_buf.at[pl.ds(0, n_x - 1)], xs.at[0])
+    got(h_buf.at[pl.ds(0, n_x - 1)], hs.at[0])
+    got(gate_v.at[pl.ds(0, serving - 2)], ygu_s.at[0])
+    got(down_v.at[pl.ds(0, n_z - 1)], ydn_s.at[0])
+
+    @pl.when(relays)
+    def _():
+        got(comb.at[pl.ds(0, n_z - 2)], tok_s.at[0])
+        got(gate_v.at[pl.ds(0, serving - 2)], gu_s.at[0])
+        got(down_v.at[pl.ds(0, n_z - 1)], dn_s.at[0])
+
+    @pl.when(jnp.logical_not(relays))
+    def _():
+        got(comb.at[pl.ds(0, n_z - 1)], tok_s.at[0])
+        got(gate_v, gu_s.at[0])
+        got(down_v.at[pl.ds(0, n_z)], dn_s.at[0])
+
     outs[0].wait()
     outs[1].wait()
     outs[2].wait()
@@ -507,9 +519,8 @@
             if pos:
                 got(ret_ref.at[0, pos], ret_r.at[pos])
         part = pl.ds(k * per, per)
-        copy = remote(ret_ref.at[0, part], ret_ref.at[1, part], fin_s.at[k], fin_r.at[k], other_core)
+        copy = remote(ret_ref.at[0, part], ret_ref.at[1, part], fin_s.at[0], fin_r.at[k], other_core)
         copy.start()
-        late_sends.append(copy)
         total = total + mixed(0, k)
         if n:
             got(ret_ref.at[1, pl.ds(backs[n - 1] * per, per)], fin_r.at[backs[n - 1]])
@@ -517,11 +528,11 @@
     got(ret_ref.at[1, pl.ds(backs[-1] * per, per)], fin_r.at[backs[-1]])
     total = total + mixed(1, backs[-1])
     mixture_ref[...] = total.astype(bf16)
-    for copy in late_sends:
-        copy.wait_send()
+    got(ret_ref.at[0], fin_s.at[0])
 
     @pl.when(relays)
     def _():
+        got(o_buf.at[pl.ds(0, n_z - 2)], ret_s.at[0])
         for n in range(2):
             got(stage_x.at[0], stage_s.at[0, n])
             got(stage_x.at[1], stage_s.at[7, n])
@@ -532,12 +543,7 @@
 
     @pl.when(jnp.logical_not(relays))
     def _():
-        got(comb.at[opposite], tok_s.at[opposite])
-        got(o_buf.at[opposite], ret_s.at[opposite])
-        for c in range(2):
-            got(stage_gu.at[c, 0], gu_s.at[opposite, c, 0])
-            got(stage_gu.at[c, 1], gu_s.at[opposite, c, 1])
-            got(stage_dn.at[c], dn_s.at[opposite, c])
+        got(o_buf.at[pl.ds(0, n_z - 1)], ret_s.at[0])
 
 
 def exchange_and_apply(tokens, routes, mix, gain, gate, up, down, sizes):
@@ -582,23 +588,23 @@
             pltpu.VMEM(up.shape, bf16),
             pltpu.VMEM(down.shape, bf16),
             dma((2,)),
+            dma((1,)),
             dma((n_z,)),
+            dma((1,)),
+            dma((n_z, 2, 2)),
+            dma((1,)),
+            dma((n_z, 2)),
+            dma((1,)),
+            dma((n_z, 2)),
+            dma((1,)),
             dma((n_z,)),
-            dma((n_z, 2, 2)),
-            dma((n_z, 2, 2)),
-            dma((n_z, 2)),
-            dma((n_z, 2)),
-            dma((n_z, 2)),
-            dma((n_z, 2)),
+            dma((1,)),
+            dma((CHUNKS, hops, 2)),
+            dma((1,)),
+            dma((CHUNKS, hops, 2)),
+            dma((1,)),
             dma((n_z,)),
-            dma((n_z,)),
-            dma((CHUNKS, hops, 2)),
-            dma((CHUNKS, hops, 2)),
-            dma((CHUNKS, hops, 2)),
-            dma((CHUNKS, hops, 2)),
-            dma((n_z,)),
-            dma((n_z,)),
-            dma((CHUNKS,)),
+            dma((1,)),
             dma((CHUNKS,)),
             dma((3,)),
             dma((3,)),
@@ -615,10 +621,40 @@
     )(tokens, routes, mix, gain, gate, up, down)
 
 
+def put_out(*refs):
+    n = (len(refs) - 1) // 3
+    ins, outs, held, sems = refs[:n], refs[n : 2 * n], refs[2 * n : 3 * n], refs[3 * n]
+    reads = [pltpu.make_async_copy(ins[i], held[i], sems.at[0, i]) for i in range(n)]
+    writes = [pltpu.make_async_copy(held[i], outs[i], sems.at[1, i]) for i in range(n)]
+    for copy in reads:
+        copy.start()
+    for read, write in zip(reads, writes):
+        read.wait()
+        write.start()
+    for copy in writes:
+        copy.wait()
+
+
+def outputs(arrays):
+    hbm = pl.BlockSpec(memory_space=pl.ANY)
+    return pl.pallas_call(
+        put_out,
+        out_shape=tuple(jax.ShapeDtypeStruct(a.shape, a.dtype) for a in arrays),
+        in_specs=[hbm] * len(arrays),
+        out_specs=tuple([hbm] * len(arrays)),
+        scratch_shapes=[pltpu.VMEM(a.shape, a.dtype) for a in arrays]
+        + [pltpu.SemaphoreType.DMA((2, len(arrays)))],
+        compiler_params=pltpu.CompilerParams(vmem_limit_bytes=67043328),
+        name="outputs",
+    )(*arrays)
+
+
 def shards(tokens, norm_gain, gate_weight, up_weight, down_weight, routes, route_weights):
     sizes = (lax.axis_size("fs_0"), lax.axis_size("tp"), lax.axis_size("grp"))
-    gate_serve, up_serve, down_serve, mixture = exchange_and_apply(
-        tokens, routes.T, route_weights.T, norm_gain[None, :], gate_weight, up_weight, down_weight, sizes
+    gate_serve, up_serve, down_serve, mixture = outputs(
+        exchange_and_apply(
+            tokens, routes.T, route_weights.T, norm_gain[None, :], gate_weight, up_weight, down_weight, sizes
+        )
     )
     return (
         gate_serve.reshape(1, -1, gate_serve.shape[2]),

time: 174 us -> 167 us (0.960)
  local copies, waits for them, and re-layouts: 4.95 us -> 0 us
  Pallas kernels: 168 us -> 166 us
    unnamed x10 -> x0, local copies, waits for them, and re-layouts: 4.95 us -> none
    pallas_call x1, Pallas kernels: 168 us -> 164 us  [exchange_and_apply(): pl.pallas_call(functools.partial(kernel, sizes), out_shape=(jax.ShapeDtyp...]
    pallas_call x0 -> x1, Pallas kernels: none -> 2.31 us  [outputs(): pl.pallas_call(put_out, out_shape=tuple((jax.ShapeDtypeStruct(a.shape, a....]
where the time goes in v4:
time: 167 us
  Pallas kernels  166 us (99%)
    pallas_call x1, Pallas kernels, exchange_and_apply(): pl.pallas_call(functools.partial(kernel, sizes), out_shape=(jax.ShapeDtyp...  164 us

profile of v4, /device:TPU:65, one launch (start us, length us, event | category | flops | bytes accessed | tf_op | source)
XLA Modules:
  0.0 167.0 jit_solution(10752631047783233968)
XLA Ops:
  0.6 163.9 %exchange_and_apply.1 = (bf16[32,64,128]{2,1,0:T(8,128)(2,1)}, bf16[32,64,128]{2,1,0:T(8,128)(2,1)}, bf16[32,32,256]{2,1,0:T(8,128)(2,1)}, bf16[384,256]{1,0:T(8,128)(2,1)}) custom-call(bf16[384,256]{1,0:T(8,128)(2,1)} %tok_ref.1, s32[2,384]{1,0:T(2,128)} %bitcast.6, f32[2,384]{1,0:T(2,128)} %bitcast.7, f32[1,64]{1,0:T(1,128)} %bitcast.8, ...), custom_call_target="tpu_custom_call" | custom-call | tf_op jit(solution)/shard_map/exchange_and_apply/pallas_call | solution.py:561
  164.5 2.3 %outputs.1 = (bf16[32,64,128]{2,1,0:T(8,128)(2,1)}, bf16[32,64,128]{2,1,0:T(8,128)(2,1)}, bf16[32,32,256]{2,1,0:T(8,128)(2,1)}, bf16[384,256]{1,0:T(8,128)(2,1)}) custom-call(bf16[32,64,128]{2,1,0:T(8,128)(2,1)} %get-tuple-element.12.refs_0_, bf16[32,64,128]{2,1,0:T(8,128)(2,1)} %get-tuple-element.13.refs_1_, ...), custom_call_target="tpu_custom_call" | custom-call | tf_op jit(solution)/shard_map/outputs/pallas_call | solution.py:640

commit v5 on v4

--- a/solution.py
+++ b/solution.py
@@ -220,23 +220,23 @@
     g_rows = pl.ds(pl.multiple_of(half * g_half, g_half), g_half)
     d_rows = pl.ds(pl.multiple_of(half * d_half, d_half), d_half)
     mate = z * 2 + 1 - core
-    send(gate_ref.at[mate], gate_v.at[me], gu_s.at[0], gu_r.at[0, 0, 0], other_core)
-    send(up_ref.at[mate], up_v.at[me], gu_s.at[0], gu_r.at[0, 0, 1], other_core)
-    send(down_ref.at[mate], down_v.at[me], dn_s.at[0], dn_r.at[0, 0], other_core)
+    send(gate_ref.at[mate], gate_v.at[me], gu_s.at[0], gu_r.at[0], other_core)
+    send(up_ref.at[mate], up_v.at[me], gu_s.at[0], gu_r.at[0], other_core)
+    send(down_ref.at[mate], down_v.at[me], dn_s.at[0], dn_r.at[0], other_core)
     def gate_up_copies(pos, c):
         cc = lax.rem(core + c, 2)
         e = ahead(pos) * 2 + cc
         device = {"fs_0": ahead(pos), "fs_1": cc}
         return (
-            remote(gate_ref.at[e, g_rows], gate_v.at[me, g_rows], gu_s.at[0], gu_r.at[pos, c, 0], device),
-            remote(up_ref.at[e, g_rows], up_v.at[me, g_rows], gu_s.at[0], gu_r.at[pos, c, 1], device),
+            remote(gate_ref.at[e, g_rows], gate_v.at[me, g_rows], gu_s.at[0], gu_r.at[pos], device),
+            remote(up_ref.at[e, g_rows], up_v.at[me, g_rows], gu_s.at[0], gu_r.at[pos], device),
         )
 
     def down_copies(pos, c):
         cc = lax.rem(core + c, 2)
         e = ahead(pos) * 2 + cc
         device = {"fs_0": ahead(pos), "fs_1": cc}
-        return (remote(down_ref.at[e, d_rows], down_v.at[me, d_rows], dn_s.at[0], dn_r.at[pos, c], device),)
+        return (remote(down_ref.at[e, d_rows], down_v.at[me, d_rows], dn_s.at[0], dn_r.at[pos], device),)
 
     def send_weights(copies_of):
         for pos in range(1, n_z - 1):
@@ -264,11 +264,10 @@
         @pl.when(relays)
         def _():
             for c in range(2):
-                n = 1 - c
                 second_leg(
-                    1 + 2 * c, stage_gu.at[c, 0], gate_v.at[origin, g_rows], gu_r.at[opposite, n, 0], leg_dest(c)
+                    1 + 2 * c, stage_gu.at[c, 0], gate_v.at[origin, g_rows], gu_r.at[opposite], leg_dest(c)
                 )
-                second_leg(2 + 2 * c, stage_gu.at[c, 1], up_v.at[origin, g_rows], gu_r.at[opposite, n, 1], leg_dest(c))
+                second_leg(2 + 2 * c, stage_gu.at[c, 1], up_v.at[origin, g_rows], gu_r.at[opposite], leg_dest(c))
 
     def send_down():
         @pl.when(relays)
@@ -282,7 +281,7 @@
         @pl.when(relays)
         def _():
             for c in range(2):
-                second_leg(5 + c, stage_dn.at[c], down_v.at[origin, d_rows], dn_r.at[opposite, 1 - c], leg_dest(c))
+                second_leg(5 + c, stage_dn.at[c], down_v.at[origin, d_rows], dn_r.at[opposite], leg_dest(c))
 
     def relay_back():
         @pl.when(relays)
@@ -301,34 +300,24 @@
         if h > 1:
             arrived(buf, k, h - 1, r_sems)
         rows = first_half if h == last else whole
-        send(buf.at[h - 1, rows], buf.at[h, rows], s_sems.at[0], r_sems.at[k, h - 1, 0], right)
+        send(buf.at[h - 1, rows], buf.at[h, rows], s_sems.at[0], r_sems.at[k, h - 1], right)
         rows = second_half if h == last else whole
-        send(buf.at[(n_x - h + 1) % n_x, rows], buf.at[n_x - h, rows], s_sems.at[0], r_sems.at[k, h - 1, 1], left)
+        send(buf.at[(n_x - h + 1) % n_x, rows], buf.at[n_x - h, rows], s_sems.at[0], r_sems.at[k, h - 1], left)
 
     def arrived(buf, k, h, r_sems):
-        last = n_x // 2
-        whole = pl.ds(k * per, per)
-        first_half, second_half = pl.ds(k * per, per // 2), pl.ds(k * per + per // 2, per // 2)
-        got(buf.at[h, first_half if h == last else whole], r_sems.at[k, h - 1, 0])
-        got(buf.at[n_x - h, second_half if h == last else whole], r_sems.at[k, h - 1, 1])
+        got(buf.at[0, pl.ds(0, per if h == n_x // 2 else 2 * per)], r_sems.at[k, h - 1])
 
     def forward_gu(k):
         for pos in range(max(1, k * per), (k + 1) * per):
-            for c in range(2):
-                cc = lax.rem(core + c, 2)
-                s = behind(pos) * 2 + cc
-                got(gate_v.at[s, g_rows], gu_r.at[pos, c, 0])
-                got(up_v.at[s, g_rows], gu_r.at[pos, c, 1])
             pair = pl.ds(behind(pos) * 2, 2)
-            send(gate_v.at[pair, g_rows], gate_v.at[pair, g_rows], ygu_s.at[0], ygu_r.at[pos, 0], y_peer)
-            send(up_v.at[pair, g_rows], up_v.at[pair, g_rows], ygu_s.at[0], ygu_r.at[pos, 1], y_peer)
+            got(gate_v.at[pair], gu_r.at[pos])
+            send(gate_v.at[pair, g_rows], gate_v.at[pair, g_rows], ygu_s.at[0], ygu_r.at[pos], y_peer)
+            send(up_v.at[pair, g_rows], up_v.at[pair, g_rows], ygu_s.at[0], ygu_r.at[pos], y_peer)
 
     def forward_dn(k):
         for pos in range(max(1, k * per), (k + 1) * per):
-            for c in range(2):
-                cc = lax.rem(core + c, 2)
-                got(down_v.at[behind(pos) * 2 + cc, d_rows], dn_r.at[pos, c])
             pair = pl.ds(behind(pos) * 2, 2)
+            got(down_v.at[pair, d_rows], dn_r.at[pos])
             send(down_v.at[pair, d_rows], down_v.at[pair, d_rows], ydn_s.at[0], ydn_r.at[pos], y_peer)
 
     def build_picks():
@@ -375,14 +364,11 @@
 
     relay_down()
 
-    o_g_rows = pl.ds(pl.multiple_of((1 - half) * g_half, g_half), g_half)
     o_d_rows = pl.ds(pl.multiple_of((1 - half) * d_half, d_half), d_half)
-    got(gate_v.at[mate], gu_r.at[0, 0, 0])
-    got(up_v.at[mate], gu_r.at[0, 0, 1])
+    got(gate_v.at[pl.ds(z * 2, 2)], gu_r.at[0])
     for pos in range(1, n_z):
         pair = pl.ds(behind(pos) * 2, 2)
-        got(gate_v.at[pair, o_g_rows], ygu_r.at[pos, 0])
-        got(up_v.at[pair, o_g_rows], ygu_r.at[pos, 1])
+        got(gate_v.at[pair], ygu_r.at[pos])
     outs = [
         pltpu.make_async_copy(gate_v, gate_out, out_sem.at[0]),
         pltpu.make_async_copy(up_v, up_out, out_sem.at[1]),
@@ -392,7 +378,7 @@
     outs[1].start()
 
     def wait_down():
-        got(down_v.at[mate], dn_r.at[0, 0])
+        got(down_v.at[mate], dn_r.at[0])
         for pos in range(1, n_z):
             got(down_v.at[pl.ds(behind(pos) * 2, 2), o_d_rows], ydn_r.at[pos])
         outs[2].start()
@@ -591,17 +577,17 @@
             dma((1,)),
             dma((n_z,)),
             dma((1,)),
-            dma((n_z, 2, 2)),
-            dma((1,)),
-            dma((n_z, 2)),
-            dma((1,)),
-            dma((n_z, 2)),
-            dma((1,)),
             dma((n_z,)),
             dma((1,)),
-            dma((CHUNKS, hops, 2)),
-            dma((1,)),
-            dma((CHUNKS, hops, 2)),
+            dma((n_z,)),
+            dma((1,)),
+            dma((n_z,)),
+            dma((1,)),
+            dma((n_z,)),
+            dma((1,)),
+            dma((CHUNKS, hops)),
+            dma((1,)),
+            dma((CHUNKS, hops)),
             dma((1,)),
             dma((n_z,)),
             dma((1,)),

time: 167 us -> 166 us (level)
  no operation moved by 1% of the time
where the time goes in v5:
time: 166 us
  Pallas kernels  165 us (99%)
    pallas_call x1, Pallas kernels, exchange_and_apply(): pl.pallas_call(functools.partial(kernel, sizes), out_shape=(jax.ShapeDtyp...  162 us

profile of v5, /device:TPU:65, one launch (start us, length us, event | category | flops | bytes accessed | tf_op | source)
XLA Modules:
  0.0 165.6 jit_solution(12207142134417708522)
XLA Ops:
  0.6 162.5 %exchange_and_apply.1 = (bf16[32,64,128]{2,1,0:T(8,128)(2,1)}, bf16[32,64,128]{2,1,0:T(8,128)(2,1)}, bf16[32,32,256]{2,1,0:T(8,128)(2,1)}, bf16[384,256]{1,0:T(8,128)(2,1)}) custom-call(bf16[384,256]{1,0:T(8,128)(2,1)} %tok_ref.1, s32[2,384]{1,0:T(2,128)} %bitcast.6, f32[2,384]{1,0:T(2,128)} %bitcast.7, f32[1,64]{1,0:T(1,128)} %bitcast.8, ...), custom_call_target="tpu_custom_call" | custom-call | tf_op jit(solution)/shard_map/exchange_and_apply/pallas_call | solution.py:547
  163.1 2.3 %outputs.1 = (bf16[32,64,128]{2,1,0:T(8,128)(2,1)}, bf16[32,64,128]{2,1,0:T(8,128)(2,1)}, bf16[32,32,256]{2,1,0:T(8,128)(2,1)}, bf16[384,256]{1,0:T(8,128)(2,1)}) custom-call(bf16[32,64,128]{2,1,0:T(8,128)(2,1)} %get-tuple-element.12.refs_0_, bf16[32,64,128]{2,1,0:T(8,128)(2,1)} %get-tuple-element.13.refs_1_, ...), custom_call_target="tpu_custom_call" | custom-call | tf_op jit(solution)/shard_map/outputs/pallas_call | solution.py:626
